TPU v7x, 32 devices: a whole 2x2x4 slice. The times are simulated.
32 devices in a mesh: fs: 4 (over y, x), tp: 8 (over z, core).
Axes of the slice: x: 2, y: 2, z: 4, core: 2. Of those that a mesh axis runs over, the one named last changes fastest.
Arguments:
- features: bfloat16 [8192, 2048], P('fs', 'tp'), may hold values from -6 to 6
- gate_cotangent: bfloat16 [8192, 4096], P('fs', 'tp'), may hold values from -0.059814453 to 0.059814453
- gate_basis: bfloat16 [2048, 128], replicated, may hold values from -0.125 to 0.125
- gate_master: float32 [2048, 4096], P('fs', 'tp'), may hold values from -6 to 6
- gate_first: float32 [128, 4096], P('fs', 'tp'), may hold values from -144 to 144
- gate_second: float32 [128, 4096], P('fs', 'tp'), may hold values from 0.2 to 4
- input_cotangent: bfloat16 [8192, 4096], P('fs', 'tp'), may hold values from -0.059814453 to 0.059814453
- input_basis: bfloat16 [2048, 128], replicated, may hold values from -0.125 to 0.125
- input_master: float32 [2048, 4096], P('fs', 'tp'), may hold values from -6 to 6
- input_first: float32 [128, 4096], P('fs', 'tp'), may hold values from -144 to 144
- input_second: float32 [128, 4096], P('fs', 'tp'), may hold values from 0.2 to 4
- state_cotangent: bfloat16 [8192, 1024], P('fs', 'tp'), may hold values from -0.059814453 to 0.059814453
- state_basis: bfloat16 [2048, 128], replicated, may hold values from -0.125 to 0.125
- state_master: float32 [2048, 1024], P('fs', 'tp'), may hold values from -6 to 6
- state_first: float32 [128, 1024], P('fs', 'tp'), may hold values from -144 to 144
- state_second: float32 [128, 1024], P('fs', 'tp'), may hold values from 0.2 to 4
Outputs:
- gate_update: float32 [2048, 4096], P('fs', 'tp')
- gate_master_next: float32 [2048, 4096], P('fs', 'tp')
- gate_first_next: float32 [128, 4096], P('fs', 'tp')
- gate_second_next: float32 [128, 4096], P('fs', 'tp')
- gate_copy: bfloat16 [2048, 4096], P(None, 'tp')
- input_update: float32 [2048, 4096], P('fs', 'tp')
- input_master_next: float32 [2048, 4096], P('fs', 'tp')
- input_first_next: float32 [128, 4096], P('fs', 'tp')
- input_second_next: float32 [128, 4096], P('fs', 'tp')
- input_copy: bfloat16 [2048, 4096], P(None, 'tp')
- state_update: float32 [2048, 1024], P('fs', 'tp')
- state_master_next: float32 [2048, 1024], P('fs', 'tp')
- state_first_next: float32 [128, 1024], P('fs', 'tp')
- state_second_next: float32 [128, 1024], P('fs', 'tp')
- state_copy: bfloat16 [2048, 1024], P(None, 'tp')
All inputs are finite; a program needn't handle non-finite values.
Results may differ from a plain program's by a relative error of at most 0.001.
Values may be sent and summed in bfloat16 or wider, within the bound.
A program may use at most 64 MiB of HBM per device.

v0:
```python
import functools

import jax
import jax.numpy as jnp
from jax import lax
from jax.experimental import pallas as pl
from jax.experimental.pallas import tpu as pltpu
from jax.sharding import PartitionSpec as P

MESH = pl.DeviceIdType.MESH
PIECES = 4
SKEW = 2
AFTER = (0, 1, 4, 7, 9, 13)
F32, BF16 = jnp.float32, jnp.bfloat16


def kernel(n, tp, *refs):
    feat_in = refs[0]
    cot_in, basis_in, master_in, first_in, second_in = (refs[1 + i : 16 : 5] for i in range(5))
    upd, mas, fir, sec, cop = (refs[16 + i : 31 : 5] for i in range(5))
    (feat, fsib, cot, basis, master, first, second, parts, up_in, dn_in, up_snd, dn_snd,
     tot, sib, proj, rs_in, direction, sums,
     load_sem, z_send, z_recv, sib_send, sib_recv, rs_send, rs_recv,
     ag_send, ag_recv, sq_send, sq_recv, bulk_send, bulk_recv) = (
        refs[31], refs[32], refs[33:36], refs[36:39], refs[39:42], refs[42:45], refs[45:48],
        *refs[48:53], refs[53], refs[54], refs[55:58], refs[58:61], refs[61:64], refs[64],
        *refs[65:])

    f, t = lax.axis_index("fs"), lax.axis_index("tp")
    zs = tp // 2
    z, c = t // 2, lax.rem(t, 2)
    mate = 2 * z + 1 - c
    half = feat.shape[0]
    width = feat.shape[1]
    rows_dev = master[0].shape[0]
    rank = proj[0].shape[0]
    rb = rank // n
    piece = half // PIECES
    count = 3 * PIECES

    def remote(src, dst, ssem, rsem, **dev):
        return pltpu.make_async_remote_copy(
            src_ref=src, dst_ref=dst, send_sem=ssem, recv_sem=rsem, device_id=dev, device_id_type=MESH
        )

    def load(src, dst, i):
        cp = pltpu.make_async_copy(src, dst, load_sem.at[i])
        cp.start()
        return cp

    my_half = pl.multiple_of(c * half, half)
    mate_half = pl.multiple_of((1 - c) * half, half)
    loads = [load(feat_in.at[pl.ds(my_half, half)], feat, 0)]
    loads += [load(basis_in[k], basis[k], 1 + k) for k in range(3)]
    loads += [load(cot_in[k], cot[k], 4 + k) for k in range(3)]
    loads += [load(first_in[k], first[k], 7 + k) for k in range(3)]
    loads += [load(second_in[k], second[k], 10 + k) for k in range(3)]
    loads += [load(master_in[k], master[k], 13 + k) for k in range(3)]

    barrier = pltpu.get_barrier_semaphore()
    for d in range(1, n):
        pl.semaphore_signal(barrier, inc=1, device_id={"fs": lax.rem(f + d, n)}, device_id_type=MESH)
    for d in range(1, tp):
        pl.semaphore_signal(barrier, inc=1, device_id={"tp": lax.rem(t + d, tp)}, device_id_type=MESH)
    pl.semaphore_wait(barrier, n + tp - 2)

    share = remote(feat_in.at[pl.ds(mate_half, half)], fsib, sib_send.at[3], sib_recv.at[3], tp=mate)
    share.start()

    @pl.when(z == 0)
    def _():
        up_in[...] = jnp.zeros_like(up_in)

    @pl.when(z == zs - 1)
    def _():
        dn_in[...] = jnp.zeros_like(dn_in)

    for cp in loads[:4]:
        cp.wait()
    mine = pl.ds(pl.multiple_of(t * width, width), width)
    theirs = pl.ds(pl.multiple_of(mate * width, width), width)
    share.wait()
    for k in range(3):
        own = jnp.dot(feat[...], basis[k][mine, :], preferred_element_type=F32)
        own += jnp.dot(fsib[...], basis[k][theirs, :], preferred_element_type=F32)
        for j in range(PIECES):
            parts[k * PIECES + j] = own[j * piece : (j + 1) * piece]

    def hop(j, has_src, has_dst, src_in, snd, lane, to):
        @pl.when((j >= 0) & (j < count))
        def _():
            jj = jnp.clip(j, 0, count - 1)
            copy = remote(snd.at[jj], src_in.at[jj], z_send.at[lane, jj], z_recv.at[lane, jj], tp=to)

            @pl.when(has_src)
            def _():
                copy.wait_recv()

            @pl.when(has_dst)
            def _():
                snd[jj] = (parts[jj] + src_in[jj].astype(F32)).astype(BF16)
                copy.start()

    above = jnp.minimum(t + 2, tp - 2 + c)
    below = jnp.maximum(t - 2, c)

    def z_step(step):
        hop(step - SKEW * z, z > 0, z < zs - 1, up_in, up_snd, 0, above)
        hop(step - SKEW * (zs - 1 - z), z < zs - 1, z > 0, dn_in, dn_snd, 1, below)

    mate_copy = [remote(tot.at[k], sib.at[k], sib_send.at[k], sib_recv.at[k], tp=mate) for k in range(3)]

    def act_total(k):
        for j in range(PIECES):
            i = k * PIECES + j
            whole = parts[i] + up_in[i].astype(F32) + dn_in[i].astype(F32)
            tot[k, j * piece : (j + 1) * piece, :] = whole.astype(BF16)
        mate_copy[k].start()

    def contract(a, b):
        return lax.dot_general(a, b, (((0,), (0,)), ((), ())), preferred_element_type=F32)

    def rows_of(i):
        return pl.ds(pl.multiple_of(i * rb, rb), rb)

    def rs_copy(k, d):
        peer = lax.rem(f + d, n)
        return remote(proj[k].at[rows_of(peer)], rs_in[k].at[d - 1], rs_send.at[k, d - 1], rs_recv.at[k, d - 1], fs=peer)

    def ag_copy(k, d, whose):
        peer = lax.rem(f + d, n)
        r = direction[k].at[rows_of(whose)]
        return remote(r, r, ag_send.at[k, d - 1], ag_recv.at[k, d - 1], fs=peer)

    def sq_copy(k, d, whose):
        peer = lax.rem(t + d, tp)
        r = sums.at[k, whose]
        return remote(r, r, sq_send.at[k, d - 1], sq_recv.at[k, d - 1], tp=peer)

    def act_project(k):
        loads[4 + k].wait()
        acc = contract(tot[k], cot[k][pl.ds(my_half, half), :])
        mate_copy[k].wait_recv()
        proj[k][...] = acc + contract(sib[k], cot[k][pl.ds(mate_half, half), :])
        for d in range(1, n):
            rs_copy(k, d).start()

    def act_moment(k):
        loads[7 + k].wait()
        loads[10 + k].wait()
        r = proj[k][rows_of(f), :]
        for d in range(1, n):
            rs_copy(k, d).wait_recv()
            r = r + rs_in[k][d - 1]
        a = 0.8 * first[k][...] + 0.2 * r
        b = 0.9 * second[k][...] + 0.1 * r * r
        fir[k][...] = a
        sec[k][...] = b
        direction[k][rows_of(f), :] = a / jnp.sqrt(b)
        for d in range(1, n):
            ag_copy(k, d, f).start()

    rows = pl.ds(pl.multiple_of(f * rows_dev, rows_dev), rows_dev)

    def act_direction(k):
        for d in range(1, n):
            ag_copy(k, d, lax.rem(f - d + n, n)).wait_recv()
        whole = direction[k][...]
        sums[k, t] = jnp.full((8, 128), jnp.sum(whole * whole), F32)
        for d in range(1, tp):
            sq_copy(k, d, t).start()
        high = whole.astype(BF16)
        low = (whole - high.astype(F32)).astype(BF16)
        base = basis[k][rows, :]
        upd[k][...] = jnp.dot(
            jnp.concatenate([base, base], axis=1),
            jnp.concatenate([high, low], axis=0),
            preferred_element_type=F32,
        )

    hrow = rows_dev // 2

    def block(k, owner, h):
        return cop[k].at[pl.ds(pl.multiple_of(owner * rows_dev + h * hrow, hrow), hrow)]

    x_peer = f + 1 - 2 * lax.rem(f, 2)
    y_peer = lax.rem(f + 2, 4)
    diag = lax.rem(x_peer + 2, 4)

    def bulk(k, lane, owner, h, to):
        b = block(k, owner, h)
        return remote(b, b, bulk_send.at[k, lane], bulk_recv.at[k, lane], fs=to)

    def act_finish(k):
        loads[13 + k].wait()
        for d in range(1, tp):
            sq_copy(k, d, lax.rem(t - d + tp, tp)).wait_recv()
        total = jnp.sum(sums[k], axis=0)[0:1, 0:1]
        entries = rank * upd[k].shape[1] * tp
        scale = lax.rsqrt(total / entries + 1e-06)
        update = upd[k][...] * scale
        upd[k][...] = update
        new = master[k][...] - 0.05 * update
        mas[k][...] = new
        cop[k][rows, :] = new.astype(BF16)
        if n == 4:
            for h in range(2):
                bulk(k, h, f, h, x_peer).start()
                bulk(k, 3 - h, f, 1 - h, y_peer).start()
        else:
            for d in range(1, n):
                for h in range(2):
                    bulk(k, 2 * (d - 1) + h, f, h, lax.rem(f + d, n)).start()

    def act_forward(k):
        if n == 4:
            bulk(k, 0, x_peer, 0, x_peer).wait_recv()
            bulk(k, 4, x_peer, 0, y_peer).start()
            bulk(k, 3, y_peer, 1, y_peer).wait_recv()
            bulk(k, 5, y_peer, 1, x_peer).start()

    def act_arrive(k):
        if n == 4:
            for i, (lane, owner, h) in enumerate(((1, x_peer, 1), (2, y_peer, 0), (4, diag, 0), (5, diag, 1))):
                bulk(k, lane, owner, h, x_peer).wait_recv()
        else:
            for d in range(1, n):
                for h in range(2):
                    owner = lax.rem(f - d + n, n)
                    lane = 2 * (d - 1) + h
                    bulk(k, lane, owner, h, owner).wait_recv()

    todo = {}
    for k in range(3):
        base = (k + 1) * PIECES - 1 + SKEW * (zs - 1)
        for after, act in zip(AFTER, (act_total, act_project, act_moment, act_direction, act_finish, act_forward)):
            todo.setdefault(base + after, []).append((act, k))
    steps = count + SKEW * (zs - 1)
    for step in range(max(max(todo) + 1, steps)):
        if step < steps:
            z_step(step)
        for act, k in sorted(todo.get(step, ()), key=lambda item: -item[1]):
            act(k)
    for k in range(3):
        act_arrive(k)

    for k in range(3):
        mate_copy[k].wait_send()
        for d in range(1, n):
            rs_copy(k, d).wait_send()
            ag_copy(k, d, f).wait_send()
        for d in range(1, tp):
            sq_copy(k, d, t).wait_send()
        if n == 4:
            for h in range(2):
                bulk(k, h, f, h, x_peer).wait_send()
                bulk(k, 3 - h, f, 1 - h, y_peer).wait_send()
            bulk(k, 4, x_peer, 0, y_peer).wait_send()
            bulk(k, 5, y_peer, 1, x_peer).wait_send()
        else:
            for d in range(1, n):
                for h in range(2):
                    bulk(k, 2 * (d - 1) + h, f, h, lax.rem(f + d, n)).wait_send()
    for j in range(count):
        @pl.when(z < zs - 1)
        def _():
            remote(up_snd.at[j], up_in.at[j], z_send.at[0, j], z_recv.at[0, j], tp=above).wait_send()

        @pl.when(z > 0)
        def _():
            remote(dn_snd.at[j], dn_in.at[j], z_send.at[1, j], z_recv.at[1, j], tp=below).wait_send()


def shards(n, tp, *args):
    features = args[0]
    cots, bases, masters, firsts, seconds = (args[1 + i : 16 : 5] for i in range(5))
    tokens, width = features.shape
    rank = bases[0].shape[1]
    rows_dev = masters[0].shape[0]
    whole_rows = rows_dev * n
    half = tokens // 2
    count = 3 * PIECES
    piece = half // PIECES
    cols = [a.shape[1] for a in cots]

    outs = []
    for k in range(3):
        outs += [
            pltpu.VMEM(masters[k].shape, F32),
            pltpu.VMEM(masters[k].shape, F32),
            pltpu.VMEM(firsts[k].shape, F32),
            pltpu.VMEM(firsts[k].shape, F32),
            pltpu.VMEM((whole_rows, cols[k]), BF16),
        ]
    like = lambda arrays: [pltpu.VMEM(a.shape, a.dtype) for a in arrays]
    lanes = 6 if n == 4 else 2 * (n - 1)
    dma = lambda *shape: pltpu.SemaphoreType.DMA(shape)
    scratch = (
        [pltpu.VMEM((half, width), BF16)] * 2
        + like(cots)
        + like(bases)
        + like(masters)
        + like(firsts)
        + like(seconds)
        + [pltpu.VMEM((count, piece, rank), F32)]
        + [pltpu.VMEM((count, piece, rank), BF16)] * 4
        + [pltpu.VMEM((3, half, rank), BF16)] * 2
        + [pltpu.VMEM((rank, w), F32) for w in cols]
        + [pltpu.VMEM((n - 1, rank // n, w), F32) for w in cols]
        + [pltpu.VMEM((rank, w), F32) for w in cols]
        + [pltpu.VMEM((3, tp, 8, 128), F32)]
        + [dma(16), dma(2, count), dma(2, count), dma(4), dma(4)]
        + [dma(3, n - 1)] * 4
        + [dma(3, tp - 1)] * 2
        + [dma(3, lanes)] * 2
    )
    return pl.pallas_call(
        functools.partial(kernel, n, tp),
        out_shape=outs,
        in_specs=[pl.BlockSpec(memory_space=pltpu.HBM)] * 16,
        out_specs=[pl.BlockSpec(memory_space=pltpu.VMEM)] * 15,
        scratch_shapes=scratch,
        compiler_params=pltpu.CompilerParams(
            collective_id=0, has_side_effects=True, vmem_limit_bytes=54 * 1024 * 1024
        ),
    )(*args)


def solution(mesh):
    split = P("fs", "tp")
    return jax.shard_map(
        functools.partial(shards, mesh.shape["fs"], mesh.shape["tp"]),
        mesh=mesh,
        in_specs=(split,) + (split, P(), split, split, split) * 3,
        out_specs=(split, split, split, split, P(None, "tp")) * 3,
        check_vma=False,
    )
```

profile of v0, /device:TPU:0, one launch (start us, length us, event | category | flops | bytes accessed | tf_op | source)
XLA Modules:
  0.0 98.5 jit_solution(17308926130512762032)
XLA Ops:
  0.7 85.4 %shard_map.271 = (f32[512,512]{1,0:T(8,128)S(1)}, f32[512,512]{1,0:T(8,128)S(1)}, f32[32,512]{1,0:T(8,128)S(1)}, f32[32,512]{1,0:T(8,128)S(1)}, bf16[2048,512]{1...) custom-call(bf16[2048,256]{1,0:T(8,128)(2,1)} %refs_0_.1, ...), custom_call_target="tpu_custom_call" | custom-call | tf_op jit(solution)/shard_map/pallas_call | solution.py:317
  86.0 1.0 copy.46
  87.0 0.6 copy.58
  87.6 0.6 copy.59
  88.2 0.6 copy.48
  88.8 0.6 copy.49
  89.5 0.6 copy.53
  90.1 0.6 copy.54
  90.7 0.7 copy.56
  91.4 0.7 copy.57
  92.1 0.8 copy.60
  92.9 1.0 copy.47
  93.9 1.0 copy.51
  94.9 1.0 copy.52
  95.8 1.3 %copy.50 = bf16[2048,512]{1,0:T(8,128)(2,1)} copy(bf16[2048,512]{1,0:T(8,128)(2,1)S(1)} %get-tuple-element.19) | data formatting | bytes 4194304
  97.2 1.3 %copy.55 = bf16[2048,512]{1,0:T(8,128)(2,1)} copy(bf16[2048,512]{1,0:T(8,128)(2,1)S(1)} %get-tuple-element.24) | data formatting | bytes 4194304
where the time goes:
time: 98.6 us; the launch traced here: 98.5 us
  Pallas kernels  85.4 us (87%)
  local copies, waits for them, and re-layouts  12.4 us (13%)
    pallas_call x1, Pallas kernels, shards(): pl.pallas_call(functools.partial(kernel, n, tp), out_shape=outs, in_specs...  85.4 us
    unnamed x15, local copies, waits for them, and re-layouts  12.4 us

commit v1 on v0

--- a/solution.py
+++ b/solution.py
@@ -269,6 +269,14 @@
         @pl.when(z > 0)
         def _():
             remote(dn_snd.at[j], dn_in.at[j], z_send.at[1, j], z_recv.at[1, j], tp=below).wait_send()
+
+
+def emit(*refs):
+    copies = [pltpu.make_async_copy(refs[i], refs[15 + i], refs[30].at[i]) for i in range(15)]
+    for cp in copies:
+        cp.start()
+    for cp in copies:
+        cp.wait()
 
 
 def shards(n, tp, *args):
@@ -314,7 +322,7 @@
         + [dma(3, tp - 1)] * 2
         + [dma(3, lanes)] * 2
     )
-    return pl.pallas_call(
+    held = pl.pallas_call(
         functools.partial(kernel, n, tp),
         out_shape=outs,
         in_specs=[pl.BlockSpec(memory_space=pltpu.HBM)] * 16,
@@ -324,6 +332,14 @@
             collective_id=0, has_side_effects=True, vmem_limit_bytes=54 * 1024 * 1024
         ),
     )(*args)
+    return pl.pallas_call(
+        emit,
+        out_shape=[jax.ShapeDtypeStruct(a.shape, a.dtype) for a in held],
+        in_specs=[pl.BlockSpec(memory_space=pltpu.VMEM)] * 15,
+        out_specs=[pl.BlockSpec(memory_space=pltpu.HBM)] * 15,
+        scratch_shapes=[pltpu.SemaphoreType.DMA((15,))],
+        compiler_params=pltpu.CompilerParams(vmem_limit_bytes=16 * 1024 * 1024),
+    )(*held)
 
 
 def solution(mesh):

time: 98.6 us -> 90 us (0.913)
  local copies, waits for them, and re-layouts: 12.4 us -> 0 us
  Pallas kernels: 85.4 us -> 89.2 us
    unnamed x15 -> x0, local copies, waits for them, and re-layouts: 12.4 us -> none
    pallas_call x0 -> x1, Pallas kernels: none -> 3.84 us  [shards(): pl.pallas_call(emit, out_shape=[jax.ShapeDtypeStruct(a.shape, a.dtype) fo...]
where the time goes in v1:
time: 90 us; the launch traced here: 89.9 us
  Pallas kernels  89.2 us (99%)
    pallas_call x1, Pallas kernels, shards(): pl.pallas_call(functools.partial(kernel, n, tp), out_shape=outs, in_specs...  85.4 us
    pallas_call x1, Pallas kernels, shards(): pl.pallas_call(emit, out_shape=[jax.ShapeDtypeStruct(a.shape, a.dtype) fo...  3.84 us

profile of v1, /device:TPU:0, one launch (start us, length us, event | category | flops | bytes accessed | tf_op | source)
XLA Modules:
  0.0 89.9 jit_solution(12602004324705699180)
XLA Ops:
  0.7 85.4 %shard_map.271 = (f32[512,512]{1,0:T(8,128)S(1)}, f32[512,512]{1,0:T(8,128)S(1)}, f32[32,512]{1,0:T(8,128)S(1)}, f32[32,512]{1,0:T(8,128)S(1)}, bf16[2048,512]{1...) custom-call(bf16[2048,256]{1,0:T(8,128)(2,1)} %refs_0_.1, ...), custom_call_target="tpu_custom_call" | custom-call | tf_op jit(solution)/shard_map/pallas_call | solution.py:325
  86.0 3.8 %shard_map.272 = (f32[512,512]{1,0:T(8,128)}, f32[512,512]{1,0:T(8,128)}, f32[32,512]{1,0:T(8,128)}, f32[32,512]{1,0:T(8,128)}, bf16[2048,512]{1,0:T(8,128)(2,1)...) custom-call(f32[512,512]{1,0:T(8,128)S(1)} %get-tuple-element.30.ref, ...), custom_call_target="tpu_custom_call" | custom-call | tf_op jit(solution)/shard_map/pallas_call | solution.py:335

commit v2 on v1

v2 whole, which is shorter than its diff:
```python
import functools

import jax
import jax.numpy as jnp
from jax import lax
from jax.experimental import pallas as pl
from jax.experimental.pallas import tpu as pltpu
from jax.sharding import PartitionSpec as P

MESH = pl.DeviceIdType.MESH
PIECES = 8
SKEW = 4
EARLY = (0, 192, 512)
EARLY_ROWS = (32, 32, 128)
LATE_PAIRS = (2, 1, 1)
START_PAIRS = 4
TAIL = (
    (-4, "relay", 0),
    (-2, "relay", 1),
    (0, "relay", 2),
    (1, "own", 4),
    (7, "total", 0),
    (8, "project", 0),
    (8.5, "relay", 3),
    (13, "moment", 0),
    (15, "total", 1),
    (16, "project", 1),
    (16.5, "relay", 4),
    (17, "tally", 0),
    (20, "direction", 0),
    (22, "moment", 1),
    (22.1, "finish", 0),
    (22.2, "send", 0, 0),
    (23, "total", 2),
    (23.2, "project", 2),
    (23.4, "send", 0, 1),
    (23.5, "tally", 1),
    (24, "direction", 1),
    (26, "finish", 1),
    (27, "forward", 0, 0),
    (27.5, "moment", 2),
    (28.1, "send", 1, 0),
    (29, "forward", 0, 1),
    (29.5, "tally", 2),
    (29.6, "direction", 2),
    (29.7, "forward", 1, 0),
    (30, "finish", 2),
    (30.1, "local", 2),
    (32, "local", 1),
    (33, "arrive", 0),
    (33, "arrive", 1),
)
PLAIN = (
    (7, "total"),
    (8, "project"),
    (13, "moment"),
    (17, "tally"),
    (21, "direction"),
    (23, "finish"),
    (23.1, "send"),
    (60, "arrive"),
)
F32, BF16 = jnp.float32, jnp.bfloat16


def plan(n, rows_dev):
    early = [min(e, rows_dev) if n == 4 else 0 for e in EARLY]
    pairs = []
    for k in (2, 1, 0):
        for at in range(0, early[k], 2 * EARLY_ROWS[k]):
            pairs.append((k, at, EARLY_ROWS[k]))
    return early, pairs


def kernel(n, tp, *refs):
    feat_in = refs[0]
    cot_in, basis_in, master_in, first_in, second_in = (refs[1 + i : 16 : 5] for i in range(5))
    upd, mas, fir, sec, cop = (refs[16 + i : 31 : 5] for i in range(5))
    (feats, fsib, cot, basis, master, first, second, parts, up_in, dn_in, up_snd, dn_snd,
     tot, sib, proj, rs_out, rs_in, direction, wide, shares, sums,
     load_sem, z_send, z_recv, sib_send, sib_recv, rs_send, rs_recv,
     ag_send, ag_recv, part_send, part_recv, sq_send, sq_recv, bulk_send, bulk_recv, early_send, early_recv) = (
        refs[31], refs[32], refs[33:36], refs[36:39], refs[39:42], refs[42:45], refs[45:48],
        *refs[48:53], refs[53], refs[54], refs[55:58], refs[58:61], refs[61:64], refs[64:67],
        refs[67:70], refs[70], refs[71], *refs[72:])

    f, t = lax.axis_index("fs"), lax.axis_index("tp")
    zs = tp // 2
    z, c = t // 2, lax.rem(t, 2)
    mate = 2 * z + 1 - c
    half = feats.shape[0] // 2
    width = feats.shape[1]
    rows_dev = master[0].shape[0]
    rank = proj[0].shape[0]
    rb = rank // n
    piece = half // PIECES
    count = 3 * PIECES
    early, pairs = plan(n, rows_dev)

    def remote(src, dst, ssem, rsem, **dev):
        return pltpu.make_async_remote_copy(
            src_ref=src, dst_ref=dst, send_sem=ssem, recv_sem=rsem, device_id=dev, device_id_type=MESH
        )

    def load(src, dst, i):
        cp = pltpu.make_async_copy(src, dst, load_sem.at[i])
        cp.start()
        return cp

    my_half = pl.multiple_of(c * half, half)
    mate_half = pl.multiple_of((1 - c) * half, half)
    loads = [load(feat_in, feats, 0)]
    loads += [load(basis_in[k], basis[k], 1 + k) for k in range(3)]
    heads = [k for k in (2, 1, 0) if early[k]]
    order = heads + [k for k in range(3) if k not in heads]
    grown = {k: load(master_in[k], master[k], 13 + k) for k in heads}
    loads += [load(cot_in[k], cot[k], 4 + k) for k in range(3)]
    loads += [load(first_in[k], first[k], 7 + k) for k in range(3)]
    loads += [load(second_in[k], second[k], 10 + k) for k in range(3)]
    grown.update({k: load(master_in[k], master[k], 13 + k) for k in order if k not in heads})
    loads += [grown[k] for k in range(3)]

    barrier = pltpu.get_barrier_semaphore()
    for d in range(1, n):
        pl.semaphore_signal(barrier, inc=1, device_id={"fs": lax.rem(f + d, n)}, device_id_type=MESH)
    for d in range(1, tp):
        pl.semaphore_signal(barrier, inc=1, device_id={"tp": lax.rem(t + d, tp)}, device_id_type=MESH)

    @pl.when(z == 0)
    def _():
        up_in[...] = jnp.zeros_like(up_in)

    @pl.when(z == zs - 1)
    def _():
        dn_in[...] = jnp.zeros_like(dn_in)

    for cp in loads[:4]:
        cp.wait()
    mine = pl.ds(pl.multiple_of(t * width, width), width)
    theirs = pl.ds(pl.multiple_of(mate * width, width), width)

    def pieces_of(k):
        return pl.ds(k * PIECES, PIECES)

    for k in range(3):
        own = jnp.dot(feats[pl.ds(my_half, half), :], basis[k][mine, :], preferred_element_type=F32)
        parts[pieces_of(k)] = own.reshape(PIECES, piece, rank)
    pl.semaphore_wait(barrier, n + tp - 2)

    share = remote(feats.at[pl.ds(mate_half, half)], fsib, sib_send.at[3], sib_recv.at[3], tp=mate)
    share.start()

    x_peer = f + 1 - 2 * lax.rem(f, 2)
    y_peer = lax.rem(f + 2, 4)
    diag = lax.rem(x_peer + 2, 4)

    def early_copy(p, lane, owner, to):
        k, at, size = pairs[p]
        r = pl.ds(at + size * (lane in (1, 3, 5)), size)
        src = master[k].at[r] if lane < 4 else wide[k].at[owner, r]
        return remote(src, wide[k].at[owner, r], early_send.at[p, lane], early_recv.at[p, lane], fs=to)

    def act_own(p):
        early_copy(p, 0, f, x_peer).start()
        early_copy(p, 3, f, y_peer).start()
        early_copy(p, 1, f, x_peer).start()
        early_copy(p, 2, f, y_peer).start()

    def act_relay(p):
        early_copy(p, 0, x_peer, x_peer).wait_recv()
        early_copy(p, 4, x_peer, y_peer).start()
        early_copy(p, 3, y_peer, y_peer).wait_recv()
        early_copy(p, 5, y_peer, x_peer).start()

    def early_arrive(p):
        for lane, owner in ((1, x_peer), (2, y_peer), (4, diag), (5, diag)):
            early_copy(p, lane, owner, x_peer).wait_recv()

    for k in heads:
        loads[13 + k].wait()
    for p in range(min(START_PAIRS, len(pairs))):
        act_own(p)

    share.wait()

    def act_join(k):
        own = jnp.dot(fsib[...], basis[k][theirs, :], preferred_element_type=F32)
        parts[pieces_of(k)] += own.reshape(PIECES, piece, rank)

    def hop(j, has_src, has_dst, src_in, snd, lane, to):
        @pl.when((j >= 0) & (j < count))
        def _():
            jj = jnp.clip(j, 0, count - 1)
            copy = remote(snd.at[jj], src_in.at[jj], z_send.at[lane, jj], z_recv.at[lane, jj], tp=to)

            @pl.when(has_src)
            def _():
                copy.wait_recv()

            @pl.when(has_dst)
            def _():
                snd[jj] = (parts[jj] + src_in[jj].astype(F32)).astype(BF16)
                copy.start()

    above = jnp.minimum(t + 2, tp - 2 + c)
    below = jnp.maximum(t - 2, c)

    def z_step(step):
        hop(step - SKEW * z, z > 0, z < zs - 1, up_in, up_snd, 0, above)
        hop(step - SKEW * (zs - 1 - z), z < zs - 1, z > 0, dn_in, dn_snd, 1, below)

    mate_copy = [remote(tot.at[k], sib.at[k], sib_send.at[k], sib_recv.at[k], tp=mate) for k in range(3)]

    def act_total(k):
        for j in range(PIECES):
            i = k * PIECES + j
            whole = parts[i] + up_in[i].astype(F32) + dn_in[i].astype(F32)
            tot[k, j * piece : (j + 1) * piece, :] = whole.astype(BF16)
        mate_copy[k].start()

    def contract(a, b):
        return lax.dot_general(a, b, (((0,), (0,)), ((), ())), preferred_element_type=F32)

    def rows_of(i):
        return pl.ds(pl.multiple_of(i * rb, rb), rb)

    def rs_copy(k, d):
        peer = lax.rem(f + d, n)
        return remote(rs_out[k].at[rows_of(peer)], rs_in[k].at[d - 1], rs_send.at[k, d - 1], rs_recv.at[k, d - 1], fs=peer)

    def ag_copy(k, d, whose):
        peer = lax.rem(f + d, n)
        r = direction[k].at[rows_of(whose)]
        return remote(r, r, ag_send.at[k, d - 1], ag_recv.at[k, d - 1], fs=peer)

    def part_copy(k, d, whose):
        peer = lax.rem(f + d, n)
        r = shares.at[k, whose]
        return remote(r, r, part_send.at[k, d - 1], part_recv.at[k, d - 1], fs=peer)

    def sq_copy(k, d, whose):
        peer = lax.rem(t + d, tp)
        r = sums.at[k, whose]
        return remote(r, r, sq_send.at[k, d - 1], sq_recv.at[k, d - 1], tp=peer)

    def act_project(k):
        loads[4 + k].wait()
        acc = contract(tot[k], cot[k][pl.ds(my_half, half), :])
        mate_copy[k].wait_recv()
        whole = acc + contract(sib[k], cot[k][pl.ds(mate_half, half), :])
        proj[k][...] = whole
        rs_out[k][...] = whole.astype(BF16)
        for d in range(1, n):
            rs_copy(k, d).start()

    def act_moment(k):
        loads[7 + k].wait()
        loads[10 + k].wait()
        r = proj[k][rows_of(f), :]
        for d in range(1, n):
            rs_copy(k, d).wait_recv()
            r = r + rs_in[k][d - 1].astype(F32)
        a = 0.8 * first[k][...] + 0.2 * r
        b = 0.9 * second[k][...] + 0.1 * r * r
        fir[k][...] = a
        sec[k][...] = b
        turned = a / jnp.sqrt(b)
        shares[k, f] = jnp.full((8, 128), jnp.sum(turned * turned), F32)
        direction[k][rows_of(f), :] = turned
        for d in range(1, n):
            part_copy(k, d, f).start()
        for d in range(1, n):
            ag_copy(k, d, f).start()

    def act_tally(k):
        for d in range(1, n):
            part_copy(k, d, lax.rem(f - d + n, n)).wait_recv()
        sums[k, t] = jnp.sum(shares[k], axis=0)
        for d in range(1, tp):
            sq_copy(k, d, t).start()

    rows = pl.ds(pl.multiple_of(f * rows_dev, rows_dev), rows_dev)

    def expand(k, base):
        whole = direction[k][...]
        high = whole.astype(BF16)
        low = (whole - high.astype(F32)).astype(BF16)
        return jnp.dot(
            jnp.concatenate([base, base], axis=1),
            jnp.concatenate([high, low], axis=0),
            preferred_element_type=F32,
        )

    def act_direction(k):
        for d in range(1, n):
            ag_copy(k, d, lax.rem(f - d + n, n)).wait_recv()
        upd[k][...] = expand(k, basis[k][rows, :])

    def scale_of(k):
        total = jnp.sum(sums[k], axis=0)[0:1, 0:1]
        entries = rank * upd[k].shape[1] * tp
        return lax.rsqrt(total / entries + 1e-06)

    late_pairs = [LATE_PAIRS[k] if n == 4 else 1 for k in range(3)]
    hrow = [(rows_dev - early[k]) // (2 * late_pairs[k]) for k in range(3)]

    def block(k, owner, h):
        size = hrow[k]
        return cop[k].at[pl.ds(pl.multiple_of(owner * rows_dev + early[k] + h * size, 8), size)]

    def bulk(k, p, lane, owner, to):
        b = block(k, owner, 2 * p + (lane in (1, 3, 5)))
        i = 6 * p + lane
        return remote(b, b, bulk_send.at[k, i], bulk_recv.at[k, i], fs=to)

    def direct(k, d, h, owner, to):
        b = block(k, owner, h)
        i = 2 * (d - 1) + h
        return remote(b, b, bulk_send.at[k, i], bulk_recv.at[k, i], fs=to)

    def settle(k, at, size, scale):
        own = pl.ds(at, size)
        update = upd[k][own, :] * scale
        upd[k][own, :] = update
        new = master[k][own, :] - 0.05 * update
        mas[k][own, :] = new
        cop[k][pl.ds(pl.multiple_of(f * rows_dev + at, 8), size), :] = new.astype(BF16)

    def act_finish(k):
        if k not in heads:
            loads[13 + k].wait()
        for d in range(1, tp):
            sq_copy(k, d, lax.rem(t - d + tp, tp)).wait_recv()

    def act_send(k, p):
        scale = scale_of(k)
        if n == 4:
            settle(k, early[k] + 2 * p * hrow[k], hrow[k], scale)
            bulk(k, p, 0, f, x_peer).start()
            settle(k, early[k] + (2 * p + 1) * hrow[k], hrow[k], scale)
            bulk(k, p, 3, f, y_peer).start()
            bulk(k, p, 1, f, x_peer).start()
            bulk(k, p, 2, f, y_peer).start()
        else:
            settle(k, 0, rows_dev, scale)
            for d in range(1, n):
                for h in range(2):
                    direct(k, d, h, f, lax.rem(f + d, n)).start()

    def act_forward(k, p):
        bulk(k, p, 0, x_peer, x_peer).wait_recv()
        bulk(k, p, 4, x_peer, y_peer).start()
        bulk(k, p, 3, y_peer, y_peer).wait_recv()
        bulk(k, p, 5, y_peer, x_peer).start()

    def act_local(k):
        for p in range(len(pairs)):
            if pairs[p][0] == k:
                early_arrive(p)
        scale = scale_of(k)
        settle(k, 0, early[k], scale)
        for owner in (x_peer, y_peer, diag):
            r = pl.ds(pl.multiple_of(owner * rows_dev, rows_dev), early[k])
            update = expand(k, basis[k][r, :]) * scale
            new = wide[k][owner] - 0.05 * update
            cop[k][r, :] = new.astype(BF16)

    def act_arrive(k):
        if n == 4:
            for p in range(late_pairs[k]):
                for lane, owner in ((1, x_peer), (2, y_peer), (4, diag), (5, diag)):
                    bulk(k, p, lane, owner, x_peer).wait_recv()
        else:
            for d in range(1, n):
                for h in range(2):
                    owner = lax.rem(f - d + n, n)
                    direct(k, d, h, owner, owner).wait_recv()

    acts = dict(
        join=act_join, relay=act_relay, own=act_own, total=act_total, project=act_project,
        moment=act_moment, tally=act_tally, direction=act_direction, finish=act_finish, send=act_send,
        forward=act_forward, local=act_local, arrive=act_arrive,
    )
    ramp = SKEW * (zs - 1)
    steps = count + ramp
    todo = [(step, 0, z_step, (step,)) for step in range(steps)]
    todo += [(0.5 if k else -1, 1, act_join, (k,)) for k in range(3)]
    if n == 4:
        todo += [(ramp + at, 2, acts[name], args) for at, name, *args in TAIL]
    else:
        for at, name in PLAIN:
            for k in range(3):
                args = (k, 0) if name == "send" else (k,)
                todo.append((ramp + at + k * PIECES, 2, acts[name], args))
    for _, _, act, args in sorted(todo, key=lambda item: item[:2]):
        act(*args)

    for p in range(len(pairs)):
        for lane in range(6):
            early_copy(p, lane, f, x_peer).wait_send()
    for k in range(3):
        mate_copy[k].wait_send()
        for d in range(1, n):
            rs_copy(k, d).wait_send()
            ag_copy(k, d, f).wait_send()
            part_copy(k, d, f).wait_send()
        for d in range(1, tp):
            sq_copy(k, d, t).wait_send()
        if n == 4:
            for p in range(late_pairs[k] if hrow[k] else 0):
                for lane in range(6):
                    bulk(k, p, lane, f, x_peer).wait_send()
        else:
            for d in range(1, n):
                for h in range(2):
                    direct(k, d, h, f, lax.rem(f + d, n)).wait_send()
    for j in range(count):
        @pl.when(z < zs - 1)
        def _():
            remote(up_snd.at[j], up_in.at[j], z_send.at[0, j], z_recv.at[0, j], tp=above).wait_send()

        @pl.when(z > 0)
        def _():
            remote(dn_snd.at[j], dn_in.at[j], z_send.at[1, j], z_recv.at[1, j], tp=below).wait_send()


def emit(*refs):
    copies = [pltpu.make_async_copy(refs[i], refs[15 + i], refs[30].at[i]) for i in range(15)]
    for cp in copies:
        cp.start()
    for cp in copies:
        cp.wait()


def shards(n, tp, *args):
    features = args[0]
    cots, bases, masters, firsts, seconds = (args[1 + i : 16 : 5] for i in range(5))
    tokens, width = features.shape
    rank = bases[0].shape[1]
    rows_dev = masters[0].shape[0]
    whole_rows = rows_dev * n
    half = tokens // 2
    count = 3 * PIECES
    piece = half // PIECES
    cols = [a.shape[1] for a in cots]

    outs = []
    for k in range(3):
        outs += [
            pltpu.VMEM(masters[k].shape, F32),
            pltpu.VMEM(masters[k].shape, F32),
            pltpu.VMEM(firsts[k].shape, F32),
            pltpu.VMEM(firsts[k].shape, F32),
            pltpu.VMEM((whole_rows, cols[k]), BF16),
        ]
    like = lambda arrays: [pltpu.VMEM(a.shape, a.dtype) for a in arrays]
    early, pairs = plan(n, rows_dev)
    lanes = 6 * max(LATE_PAIRS) if n == 4 else 2 * (n - 1)
    dma = lambda *shape: pltpu.SemaphoreType.DMA(shape)
    scratch = (
        [pltpu.VMEM((tokens, width), BF16), pltpu.VMEM((half, width), BF16)]
        + like(cots)
        + like(bases)
        + like(masters)
        + like(firsts)
        + like(seconds)
        + [pltpu.VMEM((count, piece, rank), F32)]
        + [pltpu.VMEM((count, piece, rank), BF16)] * 4
        + [pltpu.VMEM((3, half, rank), BF16)] * 2
        + [pltpu.VMEM((rank, w), F32) for w in cols]
        + [pltpu.VMEM((rank, w), BF16) for w in cols]
        + [pltpu.VMEM((n - 1, rank // n, w), BF16) for w in cols]
        + [pltpu.VMEM((rank, w), F32) for w in cols]
        + [pltpu.VMEM((n, max(e, 16), w), F32) for e, w in zip(early, cols)]
        + [pltpu.VMEM((3, n, 8, 128), F32), pltpu.VMEM((3, tp, 8, 128), F32)]
        + [dma(16), dma(2, count), dma(2, count), dma(4), dma(4)]
        + [dma(3, n - 1)] * 6
        + [dma(3, tp - 1)] * 2
        + [dma(3, lanes)] * 2
        + [dma(max(len(pairs), 1), 6)] * 2
    )
    held = pl.pallas_call(
        functools.partial(kernel, n, tp),
        out_shape=outs,
        in_specs=[pl.BlockSpec(memory_space=pltpu.HBM)] * 16,
        out_specs=[pl.BlockSpec(memory_space=pltpu.VMEM)] * 15,
        scratch_shapes=scratch,
        compiler_params=pltpu.CompilerParams(
            collective_id=0, has_side_effects=True, vmem_limit_bytes=54 * 1024 * 1024
        ),
    )(*args)
    return pl.pallas_call(
        emit,
        out_shape=[jax.ShapeDtypeStruct(a.shape, a.dtype) for a in held],
        in_specs=[pl.BlockSpec(memory_space=pltpu.VMEM)] * 15,
        out_specs=[pl.BlockSpec(memory_space=pltpu.HBM)] * 15,
        scratch_shapes=[pltpu.SemaphoreType.DMA((15,))],
        compiler_params=pltpu.CompilerParams(vmem_limit_bytes=16 * 1024 * 1024),
    )(*held)


def solution(mesh):
    split = P("fs", "tp")
    return jax.shard_map(
        functools.partial(shards, mesh.shape["fs"], mesh.shape["tp"]),
        mesh=mesh,
        in_specs=(split,) + (split, P(), split, split, split) * 3,
        out_specs=(split, split, split, split, P(None, "tp")) * 3,
        check_vma=False,
    )
```

time: 90 us -> 76.6 us (0.85)
  Pallas kernels: 89.2 us -> 75.8 us
    pallas_call x1, Pallas kernels: 85.4 us -> 71.9 us  [shards(): pl.pallas_call(functools.partial(kernel, n, tp), out_shape=outs, in_specs...]
where the time goes in v2:
time: 76.6 us; the launch traced here: 76.4 us
  Pallas kernels  75.8 us (99%)
    pallas_call x1, Pallas kernels, shards(): pl.pallas_call(functools.partial(kernel, n, tp), out_shape=outs, in_specs...  71.9 us
    pallas_call x1, Pallas kernels, shards(): pl.pallas_call(emit, out_shape=[jax.ShapeDtypeStruct(a.shape, a.dtype) fo...  3.84 us

profile of v2, /device:TPU:0, one launch (start us, length us, event | category | flops | bytes accessed | tf_op | source)
XLA Modules:
  0.0 76.4 jit_solution(2650361735469592567)
XLA Ops:
  0.7 71.9 %shard_map.271 = (f32[512,512]{1,0:T(8,128)S(1)}, f32[512,512]{1,0:T(8,128)S(1)}, f32[32,512]{1,0:T(8,128)S(1)}, f32[32,512]{1,0:T(8,128)S(1)}, bf16[2048,512]{1...) custom-call(bf16[2048,256]{1,0:T(8,128)(2,1)} %refs_0_.1, ...), custom_call_target="tpu_custom_call" | custom-call | tf_op jit(solution)/shard_map/pallas_call | solution.py:482
  72.6 3.8 %shard_map.272 = (f32[512,512]{1,0:T(8,128)}, f32[512,512]{1,0:T(8,128)}, f32[32,512]{1,0:T(8,128)}, f32[32,512]{1,0:T(8,128)}, bf16[2048,512]{1,0:T(8,128)(2,1)...) custom-call(f32[512,512]{1,0:T(8,128)S(1)} %get-tuple-element.30.ref, ...), custom_call_target="tpu_custom_call" | custom-call | tf_op jit(solution)/shard_map/pallas_call | solution.py:492

commit v3 on v2

--- a/solution.py
+++ b/solution.py
@@ -10,54 +10,87 @@
 MESH = pl.DeviceIdType.MESH
 PIECES = 8
 SKEW = 4
+SHARES = 4
+HEAD = 6
 EARLY = (0, 192, 512)
-EARLY_ROWS = (32, 32, 128)
+EARLY_ROWS = (16, 16, 64)
 LATE_PAIRS = (2, 1, 1)
-START_PAIRS = 4
+START_PAIRS = 8
+JOINS = (
+    (-3, "heads", 0),
+    (-2, "open", 0),
+    (-0.5, "join", 0, 0, 1),
+    (1.5, "join", 0, 1, 2),
+    (2.5, "join", 0, 2, 4),
+    (3.4, "open", 1),
+    (3.5, "join", 1, 0, 4),
+    (3.6, "open", 2),
+    (3.7, "join", 2, 0, 4),
+)
 TAIL = (
     (-4, "relay", 0),
-    (-2, "relay", 1),
-    (0, "relay", 2),
-    (1, "own", 4),
-    (7, "total", 0),
-    (8, "project", 0),
-    (8.5, "relay", 3),
+    (-4, "relay", 1),
+    (-2, "relay", 2),
+    (-1.9, "relay", 3),
+    (0, "relay", 4),
+    (0.1, "own", 8),
+    (5, "total", 0, 0),
+    (7, "total", 0, 1),
+    (7.1, "project", 0, 0),
+    (8, "project", 0, 1),
+    (8.5, "own", 9),
+
     (13, "moment", 0),
-    (15, "total", 1),
-    (16, "project", 1),
-    (16.5, "relay", 4),
+    (13.05, "relay", 5),
+    (13.1, "total", 1, 0),
+    (15, "total", 1, 1),
+    (15.1, "project", 1, 0),
+    (16, "project", 1, 1),
     (17, "tally", 0),
-    (20, "direction", 0),
-    (22, "moment", 1),
-    (22.1, "finish", 0),
-    (22.2, "send", 0, 0),
-    (23, "total", 2),
-    (23.2, "project", 2),
-    (23.4, "send", 0, 1),
-    (23.5, "tally", 1),
-    (24, "direction", 1),
-    (26, "finish", 1),
-    (27, "forward", 0, 0),
-    (27.5, "moment", 2),
+    (17.1, "spread", 0),
+    (17.3, "relay", 6),
+    (17.4, "relay", 7),
+    (17.5, "relay", 8),
+    (17.6, "relay", 9),
+
+    (20, "moment", 1),
+    (20.1, "direction", 0),
+    (21, "finish", 0),
+    (21.1, "send", 0, 0),
+    (21.2, "total", 2, 0),
+    (23, "total", 2, 1),
+    (23.1, "project", 2, 0),
+    (23.2, "project", 2, 1),
+    (23.3, "tally", 1),
+    (23.4, "spread", 1),
+    (23.5, "send", 0, 1),
+    (24, "forward", 0, 0),
+    (25, "moment", 2),
+    (25.5, "direction", 1),
+    (27.6, "finish", 1),
     (28.1, "send", 1, 0),
     (29, "forward", 0, 1),
     (29.5, "tally", 2),
-    (29.6, "direction", 2),
-    (29.7, "forward", 1, 0),
-    (30, "finish", 2),
-    (30.1, "local", 2),
+    (29.6, "spread", 2),
+    (30, "forward", 1, 0),
     (32, "local", 1),
+    (32.1, "direction", 2),
+    (32.2, "finish", 2),
+    (32.3, "local", 2),
+    (32.5, "drain"),
     (33, "arrive", 0),
     (33, "arrive", 1),
 )
 PLAIN = (
-    (7, "total"),
-    (8, "project"),
+    (5, "total", 0),
+    (7, "total", 1),
+    (7.1, "project", 0),
+    (8, "project", 1),
     (13, "moment"),
     (17, "tally"),
     (21, "direction"),
     (23, "finish"),
-    (23.1, "send"),
+    (23.1, "send", 0),
     (60, "arrive"),
 )
 F32, BF16 = jnp.float32, jnp.bfloat16
@@ -79,7 +112,7 @@
     (feats, fsib, cot, basis, master, first, second, parts, up_in, dn_in, up_snd, dn_snd,
      tot, sib, proj, rs_out, rs_in, direction, wide, shares, sums,
      load_sem, z_send, z_recv, sib_send, sib_recv, rs_send, rs_recv,
-     ag_send, ag_recv, part_send, part_recv, sq_send, sq_recv, bulk_send, bulk_recv, early_send, early_recv) = (
+     ag_send, ag_recv, part_send, part_recv, sq_send, sq_recv, bulk_send, bulk_recv, early_send, early_recv, early_rest) = (
         refs[31], refs[32], refs[33:36], refs[36:39], refs[39:42], refs[42:45], refs[45:48],
         *refs[48:53], refs[53], refs[54], refs[55:58], refs[58:61], refs[61:64], refs[64:67],
         refs[67:70], refs[70], refs[71], *refs[72:])
@@ -134,22 +167,20 @@
     def _():
         dn_in[...] = jnp.zeros_like(dn_in)
 
-    for cp in loads[:4]:
-        cp.wait()
+    loads[0].wait()
+    pl.semaphore_wait(barrier, n + tp - 2)
+
+    part = half // SHARES
+
+    def share(i):
+        src = feats.at[pl.ds(pl.multiple_of(mate_half + i * part, part), part)]
+        return remote(src, fsib.at[pl.ds(i * part, part)], sib_send.at[0], sib_recv.at[6 + i], tp=mate)
+
+    for i in range(SHARES):
+        share(i).start()
+
     mine = pl.ds(pl.multiple_of(t * width, width), width)
     theirs = pl.ds(pl.multiple_of(mate * width, width), width)
-
-    def pieces_of(k):
-        return pl.ds(k * PIECES, PIECES)
-
-    for k in range(3):
-        own = jnp.dot(feats[pl.ds(my_half, half), :], basis[k][mine, :], preferred_element_type=F32)
-        parts[pieces_of(k)] = own.reshape(PIECES, piece, rank)
-    pl.semaphore_wait(barrier, n + tp - 2)
-
-    share = remote(feats.at[pl.ds(mate_half, half)], fsib, sib_send.at[3], sib_recv.at[3], tp=mate)
-    share.start()
-
     x_peer = f + 1 - 2 * lax.rem(f, 2)
     y_peer = lax.rem(f + 2, 4)
     diag = lax.rem(x_peer + 2, 4)
@@ -158,7 +189,8 @@
         k, at, size = pairs[p]
         r = pl.ds(at + size * (lane in (1, 3, 5)), size)
         src = master[k].at[r] if lane < 4 else wide[k].at[owner, r]
-        return remote(src, wide[k].at[owner, r], early_send.at[p, lane], early_recv.at[p, lane], fs=to)
+        rsem = early_recv.at[p, lane // 3] if lane in (0, 3) else early_rest.at[k]
+        return remote(src, wide[k].at[owner, r], early_send.at[k], rsem, fs=to)
 
     def act_own(p):
         early_copy(p, 0, f, x_peer).start()
@@ -172,26 +204,35 @@
         early_copy(p, 3, y_peer, y_peer).wait_recv()
         early_copy(p, 5, y_peer, x_peer).start()
 
-    def early_arrive(p):
-        for lane, owner in ((1, x_peer), (2, y_peer), (4, diag), (5, diag)):
-            early_copy(p, lane, owner, x_peer).wait_recv()
-
-    for k in heads:
-        loads[13 + k].wait()
-    for p in range(min(START_PAIRS, len(pairs))):
-        act_own(p)
-
-    share.wait()
-
-    def act_join(k):
-        own = jnp.dot(fsib[...], basis[k][theirs, :], preferred_element_type=F32)
-        parts[pieces_of(k)] += own.reshape(PIECES, piece, rank)
+    def early_all(k, owners):
+        r = wide[k].at[pl.ds(0, owners)]
+        return remote(r, r, early_send.at[k], early_rest.at[k], fs=x_peer)
+
+    def act_heads(i):
+        for k in heads:
+            loads[13 + k].wait()
+        for p in range(min(START_PAIRS, len(pairs))):
+            act_own(p)
+
+    def act_open(k):
+        loads[1 + k].wait()
+        own = jnp.dot(feats[pl.ds(my_half, half), :], basis[k][mine, :], preferred_element_type=F32)
+        parts[pl.ds(k * PIECES, PIECES)] = own.reshape(PIECES, piece, rank)
+
+    def act_join(k, i, to):
+        if k == 0:
+            for q in range(i, to):
+                share(q).wait_recv()
+        size = (to - i) * part
+        own = jnp.dot(fsib[i * part : i * part + size], basis[k][theirs, :], preferred_element_type=F32)
+        at = pl.ds(k * PIECES + i * (PIECES // SHARES), (to - i) * (PIECES // SHARES))
+        parts[at] += own.reshape(size // piece, piece, rank)
 
     def hop(j, has_src, has_dst, src_in, snd, lane, to):
         @pl.when((j >= 0) & (j < count))
         def _():
             jj = jnp.clip(j, 0, count - 1)
-            copy = remote(snd.at[jj], src_in.at[jj], z_send.at[lane, jj], z_recv.at[lane, jj], tp=to)
+            copy = remote(snd.at[jj], src_in.at[jj], z_send.at[lane], z_recv.at[lane, jj], tp=to)
 
             @pl.when(has_src)
             def _():
@@ -209,14 +250,20 @@
         hop(step - SKEW * z, z > 0, z < zs - 1, up_in, up_snd, 0, above)
         hop(step - SKEW * (zs - 1 - z), z < zs - 1, z > 0, dn_in, dn_snd, 1, below)
 
-    mate_copy = [remote(tot.at[k], sib.at[k], sib_send.at[k], sib_recv.at[k], tp=mate) for k in range(3)]
-
-    def act_total(k):
-        for j in range(PIECES):
+    spans = ((0, HEAD), (HEAD, PIECES))
+
+    def mate_copy(k, p):
+        lo, hi = spans[p]
+        r = pl.ds(lo * piece, (hi - lo) * piece)
+        i = 2 * k + p
+        return remote(tot.at[k, r], sib.at[k, r], sib_send.at[1], sib_recv.at[i], tp=mate)
+
+    def act_total(k, p):
+        for j in range(*spans[p]):
             i = k * PIECES + j
             whole = parts[i] + up_in[i].astype(F32) + dn_in[i].astype(F32)
             tot[k, j * piece : (j + 1) * piece, :] = whole.astype(BF16)
-        mate_copy[k].start()
+        mate_copy(k, p).start()
 
     def contract(a, b):
         return lax.dot_general(a, b, (((0,), (0,)), ((), ())), preferred_element_type=F32)
@@ -226,28 +273,57 @@
 
     def rs_copy(k, d):
         peer = lax.rem(f + d, n)
-        return remote(rs_out[k].at[rows_of(peer)], rs_in[k].at[d - 1], rs_send.at[k, d - 1], rs_recv.at[k, d - 1], fs=peer)
+        return remote(rs_out[k].at[rows_of(peer)], rs_in[k].at[d - 1], rs_send.at[k], rs_recv.at[k], fs=peer)
 
     def ag_copy(k, d, whose):
         peer = lax.rem(f + d, n)
         r = direction[k].at[rows_of(whose)]
-        return remote(r, r, ag_send.at[k, d - 1], ag_recv.at[k, d - 1], fs=peer)
+        return remote(r, r, ag_send.at[k], ag_recv.at[k, 0], fs=peer)
 
     def part_copy(k, d, whose):
         peer = lax.rem(f + d, n)
         r = shares.at[k, whose]
-        return remote(r, r, part_send.at[k, d - 1], part_recv.at[k, d - 1], fs=peer)
+        return remote(r, r, part_send.at[k], part_recv.at[k], fs=peer)
 
     def sq_copy(k, d, whose):
         peer = lax.rem(t + d, tp)
         r = sums.at[k, whose]
-        return remote(r, r, sq_send.at[k, d - 1], sq_recv.at[k, d - 1], tp=peer)
-
-    def act_project(k):
-        loads[4 + k].wait()
-        acc = contract(tot[k], cot[k][pl.ds(my_half, half), :])
-        mate_copy[k].wait_recv()
-        whole = acc + contract(sib[k], cot[k][pl.ds(mate_half, half), :])
+        return remote(r, r, sq_send.at[k], sq_recv.at[k], tp=peer)
+
+    def rs_all(k):
+        return remote(rs_in[k], rs_in[k], rs_send.at[k], rs_recv.at[k], fs=lax.rem(f + 1, n))
+
+    def ring_copy(k, lane, owner, to):
+        size = rb // 2
+        at = pl.multiple_of(owner * rb + size * (lane in (1, 3, 5)), size)
+        r = direction[k].at[pl.ds(at, size)]
+        i = 1 + lane // 3 if lane in (0, 3) else 0
+        return remote(r, r, ag_send.at[k], ag_recv.at[k, i], fs=to)
+
+    def ag_all(k, owners):
+        r = direction[k].at[pl.ds(0, owners * rb)]
+        return remote(r, r, ag_send.at[k], ag_recv.at[k, 0], fs=lax.rem(f + 1, n))
+
+    def part_all(k):
+        r = shares.at[k, pl.ds(0, n - 1)]
+        return remote(r, r, part_send.at[k], part_recv.at[k], fs=lax.rem(f + 1, n))
+
+    def sq_all(k):
+        r = sums.at[k, pl.ds(0, tp - 1)]
+        return remote(r, r, sq_send.at[k], sq_recv.at[k], tp=lax.rem(t + 1, tp))
+
+    def act_project(k, p):
+        lo, size = spans[p][0] * piece, (spans[p][1] - spans[p][0]) * piece
+        r = pl.ds(lo, size)
+        if p == 0:
+            loads[4 + k].wait()
+        acc = contract(tot[k, r], cot[k][pl.ds(pl.multiple_of(my_half + lo, piece), size), :])
+        mate_copy(k, p).wait_recv()
+        acc += contract(sib[k, r], cot[k][pl.ds(pl.multiple_of(mate_half + lo, piece), size), :])
+        if p == 0:
+            proj[k][...] = acc
+            return
+        whole = proj[k][...] + acc
         proj[k][...] = whole
         rs_out[k][...] = whole.astype(BF16)
         for d in range(1, n):
@@ -257,8 +333,8 @@
         loads[7 + k].wait()
         loads[10 + k].wait()
         r = proj[k][rows_of(f), :]
+        rs_all(k).wait_recv()
         for d in range(1, n):
-            rs_copy(k, d).wait_recv()
             r = r + rs_in[k][d - 1].astype(F32)
         a = 0.8 * first[k][...] + 0.2 * r
         b = 0.9 * second[k][...] + 0.1 * r * r
@@ -269,12 +345,23 @@
         direction[k][rows_of(f), :] = turned
         for d in range(1, n):
             part_copy(k, d, f).start()
-        for d in range(1, n):
-            ag_copy(k, d, f).start()
+        if n == 4:
+            ring_copy(k, 0, f, x_peer).start()
+            ring_copy(k, 3, f, y_peer).start()
+            ring_copy(k, 1, f, x_peer).start()
+            ring_copy(k, 2, f, y_peer).start()
+        else:
+            for d in range(1, n):
+                ag_copy(k, d, f).start()
+
+    def act_spread(k):
+        ring_copy(k, 0, x_peer, x_peer).wait_recv()
+        ring_copy(k, 4, x_peer, y_peer).start()
+        ring_copy(k, 3, y_peer, y_peer).wait_recv()
+        ring_copy(k, 5, y_peer, x_peer).start()
 
     def act_tally(k):
-        for d in range(1, n):
-            part_copy(k, d, lax.rem(f - d + n, n)).wait_recv()
+        part_all(k).wait_recv()
         sums[k, t] = jnp.sum(shares[k], axis=0)
         for d in range(1, tp):
             sq_copy(k, d, t).start()
@@ -292,8 +379,7 @@
         )
 
     def act_direction(k):
-        for d in range(1, n):
-            ag_copy(k, d, lax.rem(f - d + n, n)).wait_recv()
+        ag_all(k, 2 if n == 4 else n - 1).wait_recv()
         upd[k][...] = expand(k, basis[k][rows, :])
 
     def scale_of(k):
@@ -310,13 +396,16 @@
 
     def bulk(k, p, lane, owner, to):
         b = block(k, owner, 2 * p + (lane in (1, 3, 5)))
-        i = 6 * p + lane
-        return remote(b, b, bulk_send.at[k, i], bulk_recv.at[k, i], fs=to)
+        i = 2 * p + 1 + lane // 3 if lane in (0, 3) else 0
+        return remote(b, b, bulk_send.at[k], bulk_recv.at[k, i], fs=to)
+
+    def bulk_all(k, count):
+        r = cop[k].at[pl.ds(0, count)]
+        return remote(r, r, bulk_send.at[k], bulk_recv.at[k, 0], fs=lax.rem(f + 1, n))
 
     def direct(k, d, h, owner, to):
         b = block(k, owner, h)
-        i = 2 * (d - 1) + h
-        return remote(b, b, bulk_send.at[k, i], bulk_recv.at[k, i], fs=to)
+        return remote(b, b, bulk_send.at[k], bulk_recv.at[k, 0], fs=to)
 
     def settle(k, at, size, scale):
         own = pl.ds(at, size)
@@ -329,8 +418,7 @@
     def act_finish(k):
         if k not in heads:
             loads[13 + k].wait()
-        for d in range(1, tp):
-            sq_copy(k, d, lax.rem(t - d + tp, tp)).wait_recv()
+        sq_all(k).wait_recv()
 
     def act_send(k, p):
         scale = scale_of(k)
@@ -354,9 +442,7 @@
         bulk(k, p, 5, y_peer, x_peer).start()
 
     def act_local(k):
-        for p in range(len(pairs)):
-            if pairs[p][0] == k:
-                early_arrive(p)
+        early_all(k, 2).wait_recv()
         scale = scale_of(k)
         settle(k, 0, early[k], scale)
         for owner in (x_peer, y_peer, diag):
@@ -366,17 +452,30 @@
             cop[k][r, :] = new.astype(BF16)
 
     def act_arrive(k):
-        if n == 4:
-            for p in range(late_pairs[k]):
-                for lane, owner in ((1, x_peer), (2, y_peer), (4, diag), (5, diag)):
-                    bulk(k, p, lane, owner, x_peer).wait_recv()
-        else:
-            for d in range(1, n):
-                for h in range(2):
-                    owner = lax.rem(f - d + n, n)
-                    direct(k, d, h, owner, owner).wait_recv()
+        bulk_all(k, 2 * (rows_dev - early[k]) if n == 4 else (n - 1) * rows_dev).wait_recv()
+
+    def act_drain():
+        remote(fsib, fsib, sib_send.at[0], sib_recv.at[0], tp=mate).wait_send()
+        remote(tot, sib, sib_send.at[1], sib_recv.at[0], tp=mate).wait_send()
+        for k in range(3):
+            if early[k]:
+                early_all(k, 3).wait_send()
+            ag_all(k, n - 1).wait_send()
+            for whole in (rs_all, part_all, sq_all):
+                whole(k).wait_send()
+
+        @pl.when(z < zs - 1)
+        def _():
+            remote(up_snd, up_in, z_send.at[0], z_recv.at[0, 0], tp=above).wait_send()
+
+        @pl.when(z > 0)
+        def _():
+            remote(dn_snd, dn_in, z_send.at[1], z_recv.at[1, 0], tp=below).wait_send()
 
     acts = dict(
+        spread=act_spread,
+        heads=act_heads, open=act_open,
+        drain=act_drain,
         join=act_join, relay=act_relay, own=act_own, total=act_total, project=act_project,
         moment=act_moment, tally=act_tally, direction=act_direction, finish=act_finish, send=act_send,
         forward=act_forward, local=act_local, arrive=act_arrive,
@@ -384,44 +483,22 @@
     ramp = SKEW * (zs - 1)
     steps = count + ramp
     todo = [(step, 0, z_step, (step,)) for step in range(steps)]
-    todo += [(0.5 if k else -1, 1, act_join, (k,)) for k in range(3)]
+    todo += [(at, 1, acts[name], args) for at, name, *args in JOINS]
     if n == 4:
         todo += [(ramp + at, 2, acts[name], args) for at, name, *args in TAIL]
     else:
-        for at, name in PLAIN:
+        for at, name, *extra in PLAIN:
             for k in range(3):
-                args = (k, 0) if name == "send" else (k,)
+                args = (k, *extra)
                 todo.append((ramp + at + k * PIECES, 2, acts[name], args))
     for _, _, act, args in sorted(todo, key=lambda item: item[:2]):
         act(*args)
 
-    for p in range(len(pairs)):
-        for lane in range(6):
-            early_copy(p, lane, f, x_peer).wait_send()
+    if n != 4:
+        act_drain()
     for k in range(3):
-        mate_copy[k].wait_send()
-        for d in range(1, n):
-            rs_copy(k, d).wait_send()
-            ag_copy(k, d, f).wait_send()
-            part_copy(k, d, f).wait_send()
-        for d in range(1, tp):
-            sq_copy(k, d, t).wait_send()
-        if n == 4:
-            for p in range(late_pairs[k] if hrow[k] else 0):
-                for lane in range(6):
-                    bulk(k, p, lane, f, x_peer).wait_send()
-        else:
-            for d in range(1, n):
-                for h in range(2):
-                    direct(k, d, h, f, lax.rem(f + d, n)).wait_send()
-    for j in range(count):
-        @pl.when(z < zs - 1)
-        def _():
-            remote(up_snd.at[j], up_in.at[j], z_send.at[0, j], z_recv.at[0, j], tp=above).wait_send()
-
-        @pl.when(z > 0)
-        def _():
-            remote(dn_snd.at[j], dn_in.at[j], z_send.at[1, j], z_recv.at[1, j], tp=below).wait_send()
+        if early[k] < rows_dev:
+            bulk_all(k, (n - 1) * (rows_dev - early[k])).wait_send()
 
 
 def emit(*refs):
@@ -455,7 +532,6 @@
         ]
     like = lambda arrays: [pltpu.VMEM(a.shape, a.dtype) for a in arrays]
     early, pairs = plan(n, rows_dev)
-    lanes = 6 * max(LATE_PAIRS) if n == 4 else 2 * (n - 1)
     dma = lambda *shape: pltpu.SemaphoreType.DMA(shape)
     scratch = (
         [pltpu.VMEM((tokens, width), BF16), pltpu.VMEM((half, width), BF16)]
@@ -473,11 +549,11 @@
         + [pltpu.VMEM((rank, w), F32) for w in cols]
         + [pltpu.VMEM((n, max(e, 16), w), F32) for e, w in zip(early, cols)]
         + [pltpu.VMEM((3, n, 8, 128), F32), pltpu.VMEM((3, tp, 8, 128), F32)]
-        + [dma(16), dma(2, count), dma(2, count), dma(4), dma(4)]
-        + [dma(3, n - 1)] * 6
-        + [dma(3, tp - 1)] * 2
-        + [dma(3, lanes)] * 2
-        + [dma(max(len(pairs), 1), 6)] * 2
+        + [dma(16), dma(2), dma(2, count), dma(2), dma(6 + SHARES)]
+        + [dma(3)] * 3
+        + [dma(3, 3)]
+        + [dma(3)] * 5
+        + [dma(3, 2 * max(LATE_PAIRS) + 1), dma(3), dma(max(len(pairs), 1), 2), dma(3)]
     )
     held = pl.pallas_call(
         functools.partial(kernel, n, tp),

time: 76.6 us -> 72.7 us (0.949)
  Pallas kernels: 75.8 us -> 71.8 us
    pallas_call x1, Pallas kernels: 71.9 us -> 68 us  [shards(): pl.pallas_call(functools.partial(kernel, n, tp), out_shape=outs, in_specs...]
where the time goes in v3:
time: 72.7 us; the launch traced here: 72.5 us
  Pallas kernels  71.8 us (99%)
    pallas_call x1, Pallas kernels, shards(): pl.pallas_call(functools.partial(kernel, n, tp), out_shape=outs, in_specs...  68 us
    pallas_call x1, Pallas kernels, shards(): pl.pallas_call(emit, out_shape=[jax.ShapeDtypeStruct(a.shape, a.dtype) fo...  3.84 us

profile of v3, /device:TPU:0, one launch (start us, length us, event | category | flops | bytes accessed | tf_op | source)
XLA Modules:
  0.0 72.5 jit_solution(2575132924329553993)
XLA Ops:
  0.7 68.0 %shard_map.271 = (f32[512,512]{1,0:T(8,128)S(1)}, f32[512,512]{1,0:T(8,128)S(1)}, f32[32,512]{1,0:T(8,128)S(1)}, f32[32,512]{1,0:T(8,128)S(1)}, bf16[2048,512]{1...) custom-call(bf16[2048,256]{1,0:T(8,128)(2,1)} %refs_0_.1, ...), custom_call_target="tpu_custom_call" | custom-call | tf_op jit(solution)/shard_map/pallas_call | solution.py:558
  68.7 3.8 %shard_map.272 = (f32[512,512]{1,0:T(8,128)}, f32[512,512]{1,0:T(8,128)}, f32[32,512]{1,0:T(8,128)}, f32[32,512]{1,0:T(8,128)}, bf16[2048,512]{1,0:T(8,128)(2,1)...) custom-call(f32[512,512]{1,0:T(8,128)S(1)} %get-tuple-element.30.ref, ...), custom_call_target="tpu_custom_call" | custom-call | tf_op jit(solution)/shard_map/pallas_call | solution.py:568

commit v4 on v3

--- a/solution.py
+++ b/solution.py
@@ -12,74 +12,90 @@
 SKEW = 4
 SHARES = 4
 HEAD = 6
-EARLY = (0, 192, 512)
-EARLY_ROWS = (16, 16, 64)
-LATE_PAIRS = (2, 1, 1)
-START_PAIRS = 8
+PAIR_ROWS = (64, 64, 256)
+BLOCK = 128
+SPAN = 120.0
 JOINS = (
-    (-3, "heads", 0),
+    (-5, "top", 2),
+    (-4, "code", 0, 0),
+    (-3, "own", 0),
     (-2, "open", 0),
     (-0.5, "join", 0, 0, 1),
     (1.5, "join", 0, 1, 2),
     (2.5, "join", 0, 2, 4),
+    (2.6, "top", 0),
+    (2.7, "code", 1, 2),
+    (2.8, "own", 1),
+    (2.9, "own", 2),
     (3.4, "open", 1),
     (3.5, "join", 1, 0, 4),
     (3.6, "open", 2),
     (3.7, "join", 2, 0, 4),
 )
 TAIL = (
-    (-4, "relay", 0),
-    (-4, "relay", 1),
-    (-2, "relay", 2),
-    (-1.9, "relay", 3),
-    (0, "relay", 4),
-    (0.1, "own", 8),
+    (-3.5, "relay", 0),
+    (-3, "code", 3, 4),
+    (-2.9, "own", 3),
+    (-1.9, "relay", 1),
+    (-1, "top", 1),
+    (0, "relay", 2),
+    (0.1, "code", 5, 6),
+    (1, "own", 4),
     (5, "total", 0, 0),
     (7, "total", 0, 1),
     (7.1, "project", 0, 0),
     (8, "project", 0, 1),
-    (8.5, "own", 9),
-
-    (13, "moment", 0),
-    (13.05, "relay", 5),
+    (8.5, "relay", 3),
+    (9, "own", 5),
+    (10, "code", 7, 8),
     (13.1, "total", 1, 0),
     (15, "total", 1, 1),
     (15.1, "project", 1, 0),
     (16, "project", 1, 1),
-    (17, "tally", 0),
-    (17.1, "spread", 0),
-    (17.3, "relay", 6),
-    (17.4, "relay", 7),
-    (17.5, "relay", 8),
-    (17.6, "relay", 9),
-
-    (20, "moment", 1),
-    (20.1, "direction", 0),
-    (21, "finish", 0),
-    (21.1, "send", 0, 0),
+    (18, "moment", 0),
+    (18.1, "relay", 4),
     (21.2, "total", 2, 0),
-    (23, "total", 2, 1),
-    (23.1, "project", 2, 0),
-    (23.2, "project", 2, 1),
-    (23.3, "tally", 1),
-    (23.4, "spread", 1),
-    (23.5, "send", 0, 1),
-    (24, "forward", 0, 0),
-    (25, "moment", 2),
-    (25.5, "direction", 1),
-    (27.6, "finish", 1),
-    (28.1, "send", 1, 0),
-    (29, "forward", 0, 1),
-    (29.5, "tally", 2),
-    (29.6, "spread", 2),
-    (30, "forward", 1, 0),
-    (32, "local", 1),
-    (32.1, "direction", 2),
-    (32.2, "finish", 2),
-    (32.3, "local", 2),
-    (32.5, "drain"),
-    (33, "arrive", 0),
-    (33, "arrive", 1),
+    (24.0, "total", 2, 1),
+    (24.1, "project", 2, 0),
+    (24.2, "project", 2, 1),
+    (24.3, "moment", 1),
+    (24.4, "tally", 0),
+    (24.5, "relay", 5),
+    (24.6, "spread", 0),
+    (24.7, "tally", 1),
+    (24.8, "moment", 2),
+    (24.9, "own", 6),
+    (25.0, "spread", 1),
+    (25.1, "tally", 2),
+    (25.2, "spread", 2),
+    (25.3, "own", 7),
+    (25.4, "direction", 0),
+    (25.5, "finish", 0),
+    (25.6, "settle", 0),
+    (25.7, "form", 0, 0),
+    (25.8, "relay", 6),
+    (25.9, "form", 0, 1),
+    (26.0, "form", 0, 2),
+    (26.1, "direction", 1),
+    (26.2, "direction", 2),
+    (26.3, "finish", 1),
+    (26.4, "finish", 2),
+    (26.5, "own", 8),
+    (26.6, "settle", 1),
+    (26.7, "settle", 2),
+    (26.8, "relay", 7),
+    (26.9, "form", 1, 0),
+    (27.0, "form", 2, 0),
+    (27.1, "form", 2, 1),
+    (27.2, "form", 2, 2),
+    (27.3, "last", 0, 0),
+    (27.4, "relay", 8),
+    (27.5, "last", 1, 4),
+    (27.6, "form", 1, 1),
+    (27.7, "form", 1, 2),
+    (27.8, "drain"),
+    (27.9, "last", 5, 6),
+    (28.0, "last", 7, 8),
 )
 PLAIN = (
     (5, "total", 0),
@@ -90,19 +106,20 @@
     (17, "tally"),
     (21, "direction"),
     (23, "finish"),
-    (23.1, "send", 0),
+    (23.1, "settle"),
+    (23.2, "send"),
     (60, "arrive"),
 )
 F32, BF16 = jnp.float32, jnp.bfloat16
 
 
 def plan(n, rows_dev):
-    early = [min(e, rows_dev) if n == 4 else 0 for e in EARLY]
     pairs = []
-    for k in (2, 1, 0):
-        for at in range(0, early[k], 2 * EARLY_ROWS[k]):
-            pairs.append((k, at, EARLY_ROWS[k]))
-    return early, pairs
+    if n == 4:
+        for k in (2, 0, 1):
+            size = min(PAIR_ROWS[k], rows_dev // 2)
+            pairs += [(k, at, size) for at in range(0, rows_dev, 2 * size)]
+    return pairs
 
 
 def kernel(n, tp, *refs):
@@ -110,12 +127,12 @@
     cot_in, basis_in, master_in, first_in, second_in = (refs[1 + i : 16 : 5] for i in range(5))
     upd, mas, fir, sec, cop = (refs[16 + i : 31 : 5] for i in range(5))
     (feats, fsib, cot, basis, master, first, second, parts, up_in, dn_in, up_snd, dn_snd,
-     tot, sib, proj, rs_out, rs_in, direction, wide, shares, sums,
+     tot, sib, proj, rs_out, rs_in, direction, wide, tops, split, shares, sums,
      load_sem, z_send, z_recv, sib_send, sib_recv, rs_send, rs_recv,
-     ag_send, ag_recv, part_send, part_recv, sq_send, sq_recv, bulk_send, bulk_recv, early_send, early_recv, early_rest) = (
+     ag_send, ag_recv, part_send, part_recv, sq_send, sq_recv, bulk_send, bulk_recv, early_send, early_recv, early_rest, top_send, top_recv) = (
         refs[31], refs[32], refs[33:36], refs[36:39], refs[39:42], refs[42:45], refs[45:48],
         *refs[48:53], refs[53], refs[54], refs[55:58], refs[58:61], refs[61:64], refs[64:67],
-        refs[67:70], refs[70], refs[71], *refs[72:])
+        refs[67:70], refs[70:73], refs[73:76], refs[76], refs[77], *refs[78:])
 
     f, t = lax.axis_index("fs"), lax.axis_index("tp")
     zs = tp // 2
@@ -128,7 +145,8 @@
     rb = rank // n
     piece = half // PIECES
     count = 3 * PIECES
-    early, pairs = plan(n, rows_dev)
+    pairs = plan(n, rows_dev)
+    block_rows = min(BLOCK, rows_dev)
 
     def remote(src, dst, ssem, rsem, **dev):
         return pltpu.make_async_remote_copy(
@@ -140,17 +158,17 @@
         cp.start()
         return cp
 
-    my_half = pl.multiple_of(c * half, half)
-    mate_half = pl.multiple_of((1 - c) * half, half)
+    side = lax.rem(c + z, 2)
+    my_half = pl.multiple_of(side * half, half)
+    mate_half = pl.multiple_of((1 - side) * half, half)
     loads = [load(feat_in, feats, 0)]
     loads += [load(basis_in[k], basis[k], 1 + k) for k in range(3)]
-    heads = [k for k in (2, 1, 0) if early[k]]
-    order = heads + [k for k in range(3) if k not in heads]
-    grown = {k: load(master_in[k], master[k], 13 + k) for k in heads}
-    loads += [load(cot_in[k], cot[k], 4 + k) for k in range(3)]
+    grown = {2: load(master_in[2], master[2], 15)}
+    loads += [load(cot_in[0], cot[0], 4)]
+    grown.update({k: load(master_in[k], master[k], 13 + k) for k in (0, 1)})
+    loads += [load(cot_in[k], cot[k], 4 + k) for k in (1, 2)]
     loads += [load(first_in[k], first[k], 7 + k) for k in range(3)]
     loads += [load(second_in[k], second[k], 10 + k) for k in range(3)]
-    grown.update({k: load(master_in[k], master[k], 13 + k) for k in order if k not in heads})
     loads += [grown[k] for k in range(3)]
 
     barrier = pltpu.get_barrier_semaphore()
@@ -185,12 +203,38 @@
     y_peer = lax.rem(f + 2, 4)
     diag = lax.rem(x_peer + 2, 4)
 
+    def peer_of(d):
+        return (diag, x_peer, y_peer)[d - 1] if n == 4 else lax.rem(f + d, n)
+
+    def top_copy(k, d):
+        r = tops[k].at[f]
+        return remote(r, r, top_send.at[k], top_recv.at[k], fs=peer_of(d))
+
+    def top_all(k):
+        r = tops[k].at[pl.ds(0, n - 1)]
+        return remote(r, r, top_send.at[k], top_recv.at[k], fs=lax.rem(f + 1, n))
+
+    def act_top(k):
+        loads[13 + k].wait()
+        tops[k][f] = jnp.maximum(jnp.max(jnp.abs(master[k][...]), axis=0, keepdims=True), 1e-30)
+        for d in range(1, n):
+            top_copy(k, d).start()
+
+    def act_code(p, to):
+        k, at, _ = pairs[p]
+        r = slice(at, pairs[to][1] + 2 * pairs[to][2])
+        value = master[k][r, :]
+        size = jnp.exp2(jnp.abs(value) * (2 * SPAN / tops[k][f]) - SPAN)
+        wide[k][f, r, :] = jnp.where(value < 0, -size, size).astype(BF16)
+
     def early_copy(p, lane, owner, to):
         k, at, size = pairs[p]
-        r = pl.ds(at + size * (lane in (1, 3, 5)), size)
-        src = master[k].at[r] if lane < 4 else wide[k].at[owner, r]
-        rsem = early_recv.at[p, lane // 3] if lane in (0, 3) else early_rest.at[k]
-        return remote(src, wide[k].at[owner, r], early_send.at[k], rsem, fs=to)
+        r = wide[k].at[owner, pl.ds(at + size * (lane in (1, 3, 5)), size)]
+        if lane in (1, 2):
+            rsem = early_rest.at[k]
+        else:
+            rsem = early_recv.at[p, {0: 0, 3: 1}.get(lane, 2)]
+        return remote(r, r, early_send.at[k], rsem, fs=to)
 
     def act_own(p):
         early_copy(p, 0, f, x_peer).start()
@@ -204,15 +248,15 @@
         early_copy(p, 3, y_peer, y_peer).wait_recv()
         early_copy(p, 5, y_peer, x_peer).start()
 
-    def early_all(k, owners):
+    def early_all(k, sem):
+        owners = 3 if sem is None else 1
         r = wide[k].at[pl.ds(0, owners)]
         return remote(r, r, early_send.at[k], early_rest.at[k], fs=x_peer)
 
-    def act_heads(i):
-        for k in heads:
-            loads[13 + k].wait()
-        for p in range(min(START_PAIRS, len(pairs))):
-            act_own(p)
+    def early_pair(p):
+        k, _, size = pairs[p]
+        r = wide[k].at[0, pl.ds(0, 2 * size)]
+        return remote(r, r, early_send.at[k], early_recv.at[p, 2], fs=x_peer)
 
     def act_open(k):
         loads[1 + k].wait()
@@ -243,8 +287,8 @@
                 snd[jj] = (parts[jj] + src_in[jj].astype(F32)).astype(BF16)
                 copy.start()
 
-    above = jnp.minimum(t + 2, tp - 2 + c)
-    below = jnp.maximum(t - 2, c)
+    above = jnp.where(z < zs - 1, t + 3 - 2 * c, mate)
+    below = jnp.where(z > 0, t - 1 - 2 * c, mate)
 
     def z_step(step):
         hop(step - SKEW * z, z > 0, z < zs - 1, up_in, up_snd, 0, above)
@@ -272,7 +316,7 @@
         return pl.ds(pl.multiple_of(i * rb, rb), rb)
 
     def rs_copy(k, d):
-        peer = lax.rem(f + d, n)
+        peer = peer_of(d)
         return remote(rs_out[k].at[rows_of(peer)], rs_in[k].at[d - 1], rs_send.at[k], rs_recv.at[k], fs=peer)
 
     def ag_copy(k, d, whose):
@@ -281,7 +325,7 @@
         return remote(r, r, ag_send.at[k], ag_recv.at[k, 0], fs=peer)
 
     def part_copy(k, d, whose):
-        peer = lax.rem(f + d, n)
+        peer = peer_of(d)
         r = shares.at[k, whose]
         return remote(r, r, part_send.at[k], part_recv.at[k], fs=peer)
 
@@ -369,17 +413,14 @@
     rows = pl.ds(pl.multiple_of(f * rows_dev, rows_dev), rows_dev)
 
     def expand(k, base):
+        return jnp.dot(jnp.concatenate([base, base], axis=1), split[k][...], preferred_element_type=F32)
+
+    def act_direction(k):
+        ag_all(k, 2 if n == 4 else n - 1).wait_recv()
         whole = direction[k][...]
         high = whole.astype(BF16)
-        low = (whole - high.astype(F32)).astype(BF16)
-        return jnp.dot(
-            jnp.concatenate([base, base], axis=1),
-            jnp.concatenate([high, low], axis=0),
-            preferred_element_type=F32,
-        )
-
-    def act_direction(k):
-        ag_all(k, 2 if n == 4 else n - 1).wait_recv()
+        split[k][:rank] = high
+        split[k][rank:] = (whole - high.astype(F32)).astype(BF16)
         upd[k][...] = expand(k, basis[k][rows, :])
 
     def scale_of(k):
@@ -387,79 +428,70 @@
         entries = rank * upd[k].shape[1] * tp
         return lax.rsqrt(total / entries + 1e-06)
 
-    late_pairs = [LATE_PAIRS[k] if n == 4 else 1 for k in range(3)]
-    hrow = [(rows_dev - early[k]) // (2 * late_pairs[k]) for k in range(3)]
-
-    def block(k, owner, h):
-        size = hrow[k]
-        return cop[k].at[pl.ds(pl.multiple_of(owner * rows_dev + early[k] + h * size, 8), size)]
-
-    def bulk(k, p, lane, owner, to):
-        b = block(k, owner, 2 * p + (lane in (1, 3, 5)))
-        i = 2 * p + 1 + lane // 3 if lane in (0, 3) else 0
-        return remote(b, b, bulk_send.at[k], bulk_recv.at[k, i], fs=to)
-
-    def bulk_all(k, count):
-        r = cop[k].at[pl.ds(0, count)]
-        return remote(r, r, bulk_send.at[k], bulk_recv.at[k, 0], fs=lax.rem(f + 1, n))
-
-    def direct(k, d, h, owner, to):
-        b = block(k, owner, h)
-        return remote(b, b, bulk_send.at[k], bulk_recv.at[k, 0], fs=to)
-
-    def settle(k, at, size, scale):
-        own = pl.ds(at, size)
-        update = upd[k][own, :] * scale
-        upd[k][own, :] = update
-        new = master[k][own, :] - 0.05 * update
-        mas[k][own, :] = new
-        cop[k][pl.ds(pl.multiple_of(f * rows_dev + at, 8), size), :] = new.astype(BF16)
-
     def act_finish(k):
-        if k not in heads:
+        if n != 4:
             loads[13 + k].wait()
         sq_all(k).wait_recv()
 
-    def act_send(k, p):
+    def act_settle(k):
+        update = upd[k][...] * scale_of(k)
+        upd[k][...] = update
+        new = master[k][...] - 0.05 * update
+        mas[k][...] = new
+        if n != 4:
+            cop[k][rows, :] = new.astype(BF16)
+
+    def direct(k, d, owner, to):
+        b = cop[k].at[pl.ds(pl.multiple_of(owner * rows_dev, rows_dev), rows_dev)]
+        return remote(b, b, bulk_send.at[k], bulk_recv.at[k], fs=to)
+
+    def bulk_all(k):
+        r = cop[k].at[pl.ds(0, (n - 1) * rows_dev)]
+        return remote(r, r, bulk_send.at[k], bulk_recv.at[k], fs=lax.rem(f + 1, n))
+
+    def act_send(k):
+        for d in range(1, n):
+            direct(k, d, f, lax.rem(f + d, n)).start()
+
+    def act_arrive(k):
+        bulk_all(k).wait_recv()
+
+    def form(k, owner, at, count):
         scale = scale_of(k)
-        if n == 4:
-            settle(k, early[k] + 2 * p * hrow[k], hrow[k], scale)
-            bulk(k, p, 0, f, x_peer).start()
-            settle(k, early[k] + (2 * p + 1) * hrow[k], hrow[k], scale)
-            bulk(k, p, 3, f, y_peer).start()
-            bulk(k, p, 1, f, x_peer).start()
-            bulk(k, p, 2, f, y_peer).start()
-        else:
-            settle(k, 0, rows_dev, scale)
-            for d in range(1, n):
-                for h in range(2):
-                    direct(k, d, h, f, lax.rem(f + d, n)).start()
-
-    def act_forward(k, p):
-        bulk(k, p, 0, x_peer, x_peer).wait_recv()
-        bulk(k, p, 4, x_peer, y_peer).start()
-        bulk(k, p, 3, y_peer, y_peer).wait_recv()
-        bulk(k, p, 5, y_peer, x_peer).start()
-
-    def act_local(k):
-        early_all(k, 2).wait_recv()
-        scale = scale_of(k)
-        settle(k, 0, early[k], scale)
-        for owner in (x_peer, y_peer, diag):
-            r = pl.ds(pl.multiple_of(owner * rows_dev, rows_dev), early[k])
-            update = expand(k, basis[k][r, :]) * scale
-            new = wide[k][owner] - 0.05 * update
-            cop[k][r, :] = new.astype(BF16)
-
-    def act_arrive(k):
-        bulk_all(k, 2 * (rows_dev - early[k]) if n == 4 else (n - 1) * rows_dev).wait_recv()
+        unit = tops[k][owner] * (0.5 / SPAN)
+
+        def body(i, carry):
+            at_i = at + i * block_rows
+            r = pl.ds(pl.multiple_of(at_i, block_rows), block_rows)
+            g = pl.ds(pl.multiple_of(owner * rows_dev + at_i, block_rows), block_rows)
+            update = expand(k, basis[k][g, :]) * scale
+            code = wide[k][owner, r, :].astype(F32)
+            size = (jnp.log2(jnp.abs(code)) + SPAN) * unit
+            cop[k][g, :] = (jnp.where(code < 0, -size, size) - 0.05 * update).astype(BF16)
+            return carry
+
+        lax.fori_loop(0, count // block_rows, body, 0)
+
+    def act_form(k, which):
+        if which == 0:
+            top_all(k).wait_recv()
+        if which == 1:
+            early_all(k, 0).wait_recv()
+        form(k, (f, x_peer, y_peer)[which], 0, rows_dev)
+
+    def act_last(p, to):
+        for q in range(p, to + 1):
+            early_pair(q).wait_recv()
+        k, at, _ = pairs[p]
+        form(k, diag, at, pairs[to][1] + 2 * pairs[to][2] - at)
 
     def act_drain():
         remote(fsib, fsib, sib_send.at[0], sib_recv.at[0], tp=mate).wait_send()
         remote(tot, sib, sib_send.at[1], sib_recv.at[0], tp=mate).wait_send()
         for k in range(3):
-            if early[k]:
-                early_all(k, 3).wait_send()
+            if n == 4:
+                early_all(k, None).wait_send()
+                top_all(k).wait_send()
             ag_all(k, n - 1).wait_send()
             for whole in (rs_all, part_all, sq_all):
                 whole(k).wait_send()
@@ -473,17 +505,15 @@
             remote(dn_snd, dn_in, z_send.at[1], z_recv.at[1, 0], tp=below).wait_send()
 
     acts = dict(
-        spread=act_spread,
-        heads=act_heads, open=act_open,
-        drain=act_drain,
-        join=act_join, relay=act_relay, own=act_own, total=act_total, project=act_project,
-        moment=act_moment, tally=act_tally, direction=act_direction, finish=act_finish, send=act_send,
-        forward=act_forward, local=act_local, arrive=act_arrive,
+        top=act_top, code=act_code, open=act_open, join=act_join, relay=act_relay, own=act_own,
+        total=act_total, project=act_project, moment=act_moment, spread=act_spread, tally=act_tally,
+        direction=act_direction, finish=act_finish, settle=act_settle, send=act_send,
+        form=act_form, last=act_last, arrive=act_arrive, drain=act_drain,
     )
     ramp = SKEW * (zs - 1)
     steps = count + ramp
     todo = [(step, 0, z_step, (step,)) for step in range(steps)]
-    todo += [(at, 1, acts[name], args) for at, name, *args in JOINS]
+    todo += [(at, 1, acts[name], args) for at, name, *args in JOINS if n == 4 or name in ("open", "join")]
     if n == 4:
         todo += [(ramp + at, 2, acts[name], args) for at, name, *args in TAIL]
     else:
@@ -497,8 +527,8 @@
     if n != 4:
         act_drain()
     for k in range(3):
-        if early[k] < rows_dev:
-            bulk_all(k, (n - 1) * (rows_dev - early[k])).wait_send()
+        if n != 4:
+            bulk_all(k).wait_send()
 
 
 def emit(*refs):
@@ -531,7 +561,8 @@
             pltpu.VMEM((whole_rows, cols[k]), BF16),
         ]
     like = lambda arrays: [pltpu.VMEM(a.shape, a.dtype) for a in arrays]
-    early, pairs = plan(n, rows_dev)
+    pairs = plan(n, rows_dev)
+    wide = (n, rows_dev) if n == 4 else (1, 16)
     dma = lambda *shape: pltpu.SemaphoreType.DMA(shape)
     scratch = (
         [pltpu.VMEM((tokens, width), BF16), pltpu.VMEM((half, width), BF16)]
@@ -547,13 +578,15 @@
         + [pltpu.VMEM((rank, w), BF16) for w in cols]
         + [pltpu.VMEM((n - 1, rank // n, w), BF16) for w in cols]
         + [pltpu.VMEM((rank, w), F32) for w in cols]
-        + [pltpu.VMEM((n, max(e, 16), w), F32) for e, w in zip(early, cols)]
+        + [pltpu.VMEM((*wide, w), BF16) for w in cols]
+        + [pltpu.VMEM((n, 1, w), F32) for w in cols]
+        + [pltpu.VMEM((2 * rank, w), BF16) for w in cols]
         + [pltpu.VMEM((3, n, 8, 128), F32), pltpu.VMEM((3, tp, 8, 128), F32)]
         + [dma(16), dma(2), dma(2, count), dma(2), dma(6 + SHARES)]
         + [dma(3)] * 3
         + [dma(3, 3)]
         + [dma(3)] * 5
-        + [dma(3, 2 * max(LATE_PAIRS) + 1), dma(3), dma(max(len(pairs), 1), 2), dma(3)]
+        + [dma(3), dma(3), dma(max(len(pairs), 1), 3)] + [dma(3)] * 3
     )
     held = pl.pallas_call(
         functools.partial(kernel, n, tp),

time: 72.7 us -> 60.9 us (0.84)
  Pallas kernels: 71.8 us -> 60 us
    pallas_call x1, Pallas kernels: 68 us -> 56.2 us  [shards(): pl.pallas_call(functools.partial(kernel, n, tp), out_shape=outs, in_specs...]
where the time goes in v4:
time: 60.9 us; the launch traced here: 60.7 us
  Pallas kernels  60 us (99%)
  between operations  0.66 us (1%)
    pallas_call x1, Pallas kernels, shards(): pl.pallas_call(functools.partial(kernel, n, tp), out_shape=outs, in_specs...  56.2 us
    pallas_call x1, Pallas kernels, shards(): pl.pallas_call(emit, out_shape=[jax.ShapeDtypeStruct(a.shape, a.dtype) fo...  3.84 us

profile of v4, /device:TPU:0, one launch (start us, length us, event | category | flops | bytes accessed | tf_op | source)
XLA Modules:
  0.0 60.7 jit_solution(12723989693457530489)
XLA Ops:
  0.7 56.2 %shard_map.271 = (f32[512,512]{1,0:T(8,128)S(1)}, f32[512,512]{1,0:T(8,128)S(1)}, f32[32,512]{1,0:T(8,128)S(1)}, f32[32,512]{1,0:T(8,128)S(1)}, bf16[2048,512]{1...) custom-call(bf16[2048,256]{1,0:T(8,128)(2,1)} %refs_0_.1, ...), custom_call_target="tpu_custom_call" | custom-call | tf_op jit(solution)/shard_map/pallas_call | solution.py:591
  56.9 3.8 %shard_map.272 = (f32[512,512]{1,0:T(8,128)}, f32[512,512]{1,0:T(8,128)}, f32[32,512]{1,0:T(8,128)}, f32[32,512]{1,0:T(8,128)}, bf16[2048,512]{1,0:T(8,128)(2,1)...) custom-call(f32[512,512]{1,0:T(8,128)S(1)} %get-tuple-element.30.ref, ...), custom_call_target="tpu_custom_call" | custom-call | tf_op jit(solution)/shard_map/pallas_call | solution.py:601

commit v5 on v4

--- a/solution.py
+++ b/solution.py
@@ -40,62 +40,62 @@
     (-1, "top", 1),
     (0, "relay", 2),
     (0.1, "code", 5, 6),
-    (1, "own", 4),
     (5, "total", 0, 0),
     (7, "total", 0, 1),
     (7.1, "project", 0, 0),
     (8, "project", 0, 1),
+    (8.2, "own", 4),
     (8.5, "relay", 3),
-    (9, "own", 5),
     (10, "code", 7, 8),
     (13.1, "total", 1, 0),
+    (14.5, "moment", 0),
     (15, "total", 1, 1),
     (15.1, "project", 1, 0),
     (16, "project", 1, 1),
-    (18, "moment", 0),
-    (18.1, "relay", 4),
+    (16.5, "own", 5),
+    (20.5, "tally", 0),
+    (20.6, "spread", 0),
+    (20.7, "relay", 4),
     (21.2, "total", 2, 0),
     (24.0, "total", 2, 1),
     (24.1, "project", 2, 0),
     (24.2, "project", 2, 1),
     (24.3, "moment", 1),
-    (24.4, "tally", 0),
-    (24.5, "relay", 5),
-    (24.6, "spread", 0),
-    (24.7, "tally", 1),
-    (24.8, "moment", 2),
-    (24.9, "own", 6),
-    (25.0, "spread", 1),
-    (25.1, "tally", 2),
-    (25.2, "spread", 2),
+    (24.4, "relay", 5),
+    (24.5, "own", 6),
+    (24.6, "direction", 0),
+    (24.7, "finish", 0),
+    (24.8, "settle", 0),
+    (24.9, "form", 0, 0),
+    (25.0, "moment", 2),
+    (25.1, "tally", 1),
+    (25.2, "spread", 1),
     (25.3, "own", 7),
-    (25.4, "direction", 0),
-    (25.5, "finish", 0),
-    (25.6, "settle", 0),
-    (25.7, "form", 0, 0),
-    (25.8, "relay", 6),
-    (25.9, "form", 0, 1),
-    (26.0, "form", 0, 2),
-    (26.1, "direction", 1),
-    (26.2, "direction", 2),
-    (26.3, "finish", 1),
-    (26.4, "finish", 2),
-    (26.5, "own", 8),
-    (26.6, "settle", 1),
-    (26.7, "settle", 2),
-    (26.8, "relay", 7),
-    (26.9, "form", 1, 0),
-    (27.0, "form", 2, 0),
-    (27.1, "form", 2, 1),
-    (27.2, "form", 2, 2),
+    (25.4, "form", 0, 1),
+    (25.5, "tally", 2),
+    (25.6, "spread", 2),
+    (25.7, "relay", 6),
+    (25.8, "own", 8),
+    (25.9, "form", 0, 2),
+    (26.0, "direction", 1),
+    (26.1, "finish", 1),
+    (26.2, "settle", 1),
+    (26.3, "relay", 7),
+    (26.4, "last", 1, 4),
+    (26.5, "form", 1, 0),
+    (26.6, "direction", 2),
+    (26.7, "finish", 2),
+    (26.8, "settle", 2),
+    (26.9, "form", 2, 0),
+    (27.0, "form", 2, 1),
+    (27.1, "form", 2, 2),
+    (27.2, "relay", 8),
     (27.3, "last", 0, 0),
-    (27.4, "relay", 8),
-    (27.5, "last", 1, 4),
-    (27.6, "form", 1, 1),
-    (27.7, "form", 1, 2),
-    (27.8, "drain"),
-    (27.9, "last", 5, 6),
-    (28.0, "last", 7, 8),
+    (27.4, "form", 1, 1),
+    (27.5, "form", 1, 2),
+    (27.6, "drain"),
+    (27.7, "last", 5, 6),
+    (27.8, "last", 7, 8),
 )
 PLAIN = (
     (5, "total", 0),
@@ -113,6 +113,21 @@
 F32, BF16 = jnp.float32, jnp.bfloat16
 
 
+def peak(value):
+    return jnp.maximum(jnp.max(jnp.abs(value), axis=0, keepdims=True), 1e-30)
+
+
+def coded(value, top):
+    size = jnp.exp2(jnp.abs(value) * (2 * SPAN / top) - SPAN)
+    return jnp.where(value < 0, -size, size).astype(BF16)
+
+
+def decoded(code, top):
+    code = code.astype(F32)
+    size = (jnp.log2(jnp.abs(code)) + SPAN) * (top * (0.5 / SPAN))
+    return jnp.where(code < 0, -size, size)
+
+
 def plan(n, rows_dev):
     pairs = []
     if n == 4:
@@ -127,12 +142,12 @@
     cot_in, basis_in, master_in, first_in, second_in = (refs[1 + i : 16 : 5] for i in range(5))
     upd, mas, fir, sec, cop = (refs[16 + i : 31 : 5] for i in range(5))
     (feats, fsib, cot, basis, master, first, second, parts, up_in, dn_in, up_snd, dn_snd,
-     tot, sib, proj, rs_out, rs_in, direction, wide, tops, split, shares, sums,
+     tot, sib, proj, rs_out, rs_in, direction, wide, tops, split, marks, sums,
      load_sem, z_send, z_recv, sib_send, sib_recv, rs_send, rs_recv,
      ag_send, ag_recv, part_send, part_recv, sq_send, sq_recv, bulk_send, bulk_recv, early_send, early_recv, early_rest, top_send, top_recv) = (
         refs[31], refs[32], refs[33:36], refs[36:39], refs[39:42], refs[42:45], refs[45:48],
         *refs[48:53], refs[53], refs[54], refs[55:58], refs[58:61], refs[61:64], refs[64:67],
-        refs[67:70], refs[70:73], refs[73:76], refs[76], refs[77], *refs[78:])
+        refs[67:70], refs[70:73], refs[73:76], refs[76:79], refs[79], *refs[80:])
 
     f, t = lax.axis_index("fs"), lax.axis_index("tp")
     zs = tp // 2
@@ -216,16 +231,14 @@
 
     def act_top(k):
         loads[13 + k].wait()
-        tops[k][f] = jnp.maximum(jnp.max(jnp.abs(master[k][...]), axis=0, keepdims=True), 1e-30)
+        tops[k][f] = peak(master[k][...])
         for d in range(1, n):
             top_copy(k, d).start()
 
     def act_code(p, to):
         k, at, _ = pairs[p]
         r = slice(at, pairs[to][1] + 2 * pairs[to][2])
-        value = master[k][r, :]
-        size = jnp.exp2(jnp.abs(value) * (2 * SPAN / tops[k][f]) - SPAN)
-        wide[k][f, r, :] = jnp.where(value < 0, -size, size).astype(BF16)
+        wide[k][f, r, :] = coded(master[k][r, :], tops[k][f])
 
     def early_copy(p, lane, owner, to):
         k, at, size = pairs[p]
@@ -326,7 +339,7 @@
 
     def part_copy(k, d, whose):
         peer = peer_of(d)
-        r = shares.at[k, whose]
+        r = marks[k].at[whose]
         return remote(r, r, part_send.at[k], part_recv.at[k], fs=peer)
 
     def sq_copy(k, d, whose):
@@ -349,7 +362,7 @@
         return remote(r, r, ag_send.at[k], ag_recv.at[k, 0], fs=lax.rem(f + 1, n))
 
     def part_all(k):
-        r = shares.at[k, pl.ds(0, n - 1)]
+        r = marks[k].at[pl.ds(0, n - 1)]
         return remote(r, r, part_send.at[k], part_recv.at[k], fs=lax.rem(f + 1, n))
 
     def sq_all(k):
@@ -385,8 +398,10 @@
         fir[k][...] = a
         sec[k][...] = b
         turned = a / jnp.sqrt(b)
-        shares[k, f] = jnp.full((8, 128), jnp.sum(turned * turned), F32)
-        direction[k][rows_of(f), :] = turned
+        top = peak(turned)
+        marks[k][f, :, :128] = jnp.full((1, 128), jnp.sum(turned * turned), F32)
+        marks[k][f, :, 128:] = top
+        direction[k][rows_of(f), :] = coded(turned, top)
         for d in range(1, n):
             part_copy(k, d, f).start()
         if n == 4:
@@ -406,7 +421,7 @@
 
     def act_tally(k):
         part_all(k).wait_recv()
-        sums[k, t] = jnp.sum(shares[k], axis=0)
+        sums[k, t] = jnp.broadcast_to(jnp.sum(marks[k][:, :, :128], axis=0), (8, 128))
         for d in range(1, tp):
             sq_copy(k, d, t).start()
 
@@ -417,10 +432,11 @@
 
     def act_direction(k):
         ag_all(k, 2 if n == 4 else n - 1).wait_recv()
-        whole = direction[k][...]
-        high = whole.astype(BF16)
-        split[k][:rank] = high
-        split[k][rank:] = (whole - high.astype(F32)).astype(BF16)
+        for i in range(n):
+            whole = decoded(direction[k][i * rb : (i + 1) * rb], marks[k][i, :, 128:])
+            high = whole.astype(BF16)
+            split[k][i * rb : (i + 1) * rb] = high
+            split[k][rank + i * rb : rank + (i + 1) * rb] = (whole - high.astype(F32)).astype(BF16)
         upd[k][...] = expand(k, basis[k][rows, :])
 
     def scale_of(k):
@@ -458,16 +474,14 @@
 
     def form(k, owner, at, count):
         scale = scale_of(k)
-        unit = tops[k][owner] * (0.5 / SPAN)
+        top = tops[k][owner]
 
         def body(i, carry):
             at_i = at + i * block_rows
             r = pl.ds(pl.multiple_of(at_i, block_rows), block_rows)
             g = pl.ds(pl.multiple_of(owner * rows_dev + at_i, block_rows), block_rows)
             update = expand(k, basis[k][g, :]) * scale
-            code = wide[k][owner, r, :].astype(F32)
-            size = (jnp.log2(jnp.abs(code)) + SPAN) * unit
-            cop[k][g, :] = (jnp.where(code < 0, -size, size) - 0.05 * update).astype(BF16)
+            cop[k][g, :] = (decoded(wide[k][owner, r, :], top) - 0.05 * update).astype(BF16)
             return carry
 
         lax.fori_loop(0, count // block_rows, body, 0)
@@ -577,11 +591,12 @@
         + [pltpu.VMEM((rank, w), F32) for w in cols]
         + [pltpu.VMEM((rank, w), BF16) for w in cols]
         + [pltpu.VMEM((n - 1, rank // n, w), BF16) for w in cols]
-        + [pltpu.VMEM((rank, w), F32) for w in cols]
+        + [pltpu.VMEM((rank, w), BF16) for w in cols]
         + [pltpu.VMEM((*wide, w), BF16) for w in cols]
         + [pltpu.VMEM((n, 1, w), F32) for w in cols]
         + [pltpu.VMEM((2 * rank, w), BF16) for w in cols]
-        + [pltpu.VMEM((3, n, 8, 128), F32), pltpu.VMEM((3, tp, 8, 128), F32)]
+        + [pltpu.VMEM((n, 1, 128 + w), F32) for w in cols]
+        + [pltpu.VMEM((3, tp, 8, 128), F32)]
         + [dma(16), dma(2), dma(2, count), dma(2), dma(6 + SHARES)]
         + [dma(3)] * 3
         + [dma(3, 3)]

time: 60.9 us -> 58.8 us (0.966)
  Pallas kernels: 60 us -> 58 us
    pallas_call x1, Pallas kernels: 56.2 us -> 54.2 us  [shards(): pl.pallas_call(functools.partial(kernel, n, tp), out_shape=outs, in_specs...]
where the time goes in v5:
time: 58.8 us; the launch traced here: 58.7 us
  Pallas kernels  58 us (99%)
  between operations  0.66 us (1%)
    pallas_call x1, Pallas kernels, shards(): pl.pallas_call(functools.partial(kernel, n, tp), out_shape=outs, in_specs...  54.2 us
    pallas_call x1, Pallas kernels, shards(): pl.pallas_call(emit, out_shape=[jax.ShapeDtypeStruct(a.shape, a.dtype) fo...  3.84 us

profile of v5, /device:TPU:0, one launch (start us, length us, event | category | flops | bytes accessed | tf_op | source)
XLA Modules:
  0.0 58.7 jit_solution(5372719119492026862)
XLA Ops:
  0.7 54.2 %shard_map.271 = (f32[512,512]{1,0:T(8,128)S(1)}, f32[512,512]{1,0:T(8,128)S(1)}, f32[32,512]{1,0:T(8,128)S(1)}, f32[32,512]{1,0:T(8,128)S(1)}, bf16[2048,512]{1...) custom-call(bf16[2048,256]{1,0:T(8,128)(2,1)} %refs_0_.1, ...), custom_call_target="tpu_custom_call" | custom-call | tf_op jit(solution)/shard_map/pallas_call | solution.py:606
  54.8 3.8 %shard_map.272 = (f32[512,512]{1,0:T(8,128)}, f32[512,512]{1,0:T(8,128)}, f32[32,512]{1,0:T(8,128)}, f32[32,512]{1,0:T(8,128)}, bf16[2048,512]{1,0:T(8,128)(2,1)...) custom-call(f32[512,512]{1,0:T(8,128)S(1)} %get-tuple-element.30.ref, ...), custom_call_target="tpu_custom_call" | custom-call | tf_op jit(solution)/shard_map/pallas_call | solution.py:616

commit v6 on v5

--- a/solution.py
+++ b/solution.py
@@ -19,6 +19,7 @@
     (-5, "top", 2),
     (-4, "code", 0, 0),
     (-3, "own", 0),
+    (-2.5, "share"),
     (-2, "open", 0),
     (-0.5, "join", 0, 0, 1),
     (1.5, "join", 0, 1, 2),
@@ -62,7 +63,7 @@
     (24.2, "project", 2, 1),
     (24.3, "moment", 1),
     (24.4, "relay", 5),
-    (24.5, "own", 6),
+    (24.5, "own", 6, 0),
     (24.6, "direction", 0),
     (24.7, "finish", 0),
     (24.8, "settle", 0),
@@ -70,32 +71,36 @@
     (25.0, "moment", 2),
     (25.1, "tally", 1),
     (25.2, "spread", 1),
-    (25.3, "own", 7),
-    (25.4, "form", 0, 1),
-    (25.5, "tally", 2),
-    (25.6, "spread", 2),
-    (25.7, "relay", 6),
-    (25.8, "own", 8),
-    (25.9, "form", 0, 2),
-    (26.0, "direction", 1),
-    (26.1, "finish", 1),
-    (26.2, "settle", 1),
-    (26.3, "relay", 7),
-    (26.4, "last", 1, 4),
-    (26.5, "form", 1, 0),
-    (26.6, "direction", 2),
-    (26.7, "finish", 2),
-    (26.8, "settle", 2),
-    (26.9, "form", 2, 0),
-    (27.0, "form", 2, 1),
-    (27.1, "form", 2, 2),
-    (27.2, "relay", 8),
-    (27.3, "last", 0, 0),
-    (27.4, "form", 1, 1),
-    (27.5, "form", 1, 2),
-    (27.6, "drain"),
-    (27.7, "last", 5, 6),
-    (27.8, "last", 7, 8),
+    (25.3, "own", 6, 1),
+    (25.4, "own", 7, 0),
+    (25.5, "form", 0, 1),
+    (25.6, "form", 0, 2),
+    (25.7, "last", 1, 4),
+    (25.8, "tally", 2),
+    (25.9, "spread", 2),
+    (26.0, "own", 7, 1),
+    (26.1, "relay", 6),
+    (26.2, "own", 8, 0),
+    (26.3, "direction", 1),
+    (26.4, "finish", 1),
+    (26.5, "settle", 1),
+    (26.6, "form", 1, 0),
+    (26.7, "own", 8, 1),
+    (26.8, "relay", 7),
+    (26.9, "direction", 2),
+    (27.0, "finish", 2),
+    (27.1, "settle", 2),
+    (27.2, "form", 2, 0),
+    (27.3, "form", 2, 1),
+    (27.4, "relay", 8),
+    (27.5, "form", 2, 2),
+    (27.6, "last", 0, 0),
+    (27.7, "form", 1, 1),
+    (27.8, "form", 1, 2),
+    (27.9, "drain"),
+    (28.0, "last", 5, 6),
+    (28.1, "last", 7, 7),
+    (99, "last", 8, 8),
 )
 PLAIN = (
     (5, "total", 0),
@@ -176,9 +181,9 @@
     side = lax.rem(c + z, 2)
     my_half = pl.multiple_of(side * half, half)
     mate_half = pl.multiple_of((1 - side) * half, half)
+    grown = {2: load(master_in[2], master[2], 15)}
     loads = [load(feat_in, feats, 0)]
     loads += [load(basis_in[k], basis[k], 1 + k) for k in range(3)]
-    grown = {2: load(master_in[2], master[2], 15)}
     loads += [load(cot_in[0], cot[0], 4)]
     grown.update({k: load(master_in[k], master[k], 13 + k) for k in (0, 1)})
     loads += [load(cot_in[k], cot[k], 4 + k) for k in (1, 2)]
@@ -200,7 +205,6 @@
     def _():
         dn_in[...] = jnp.zeros_like(dn_in)
 
-    loads[0].wait()
     pl.semaphore_wait(barrier, n + tp - 2)
 
     part = half // SHARES
@@ -209,8 +213,10 @@
         src = feats.at[pl.ds(pl.multiple_of(mate_half + i * part, part), part)]
         return remote(src, fsib.at[pl.ds(i * part, part)], sib_send.at[0], sib_recv.at[6 + i], tp=mate)
 
-    for i in range(SHARES):
-        share(i).start()
+    def act_share():
+        loads[0].wait()
+        for i in range(SHARES):
+            share(i).start()
 
     mine = pl.ds(pl.multiple_of(t * width, width), width)
     theirs = pl.ds(pl.multiple_of(mate * width, width), width)
@@ -246,19 +252,20 @@
         if lane in (1, 2):
             rsem = early_rest.at[k]
         else:
-            rsem = early_recv.at[p, {0: 0, 3: 1}.get(lane, 2)]
+            rsem = early_recv.at[p, lane // 4]
         return remote(r, r, early_send.at[k], rsem, fs=to)
 
-    def act_own(p):
-        early_copy(p, 0, f, x_peer).start()
-        early_copy(p, 3, f, y_peer).start()
-        early_copy(p, 1, f, x_peer).start()
-        early_copy(p, 2, f, y_peer).start()
+    def act_own(p, *halves):
+        if 0 in (halves or (0,)):
+            early_copy(p, 0, f, x_peer).start()
+            early_copy(p, 3, f, y_peer).start()
+        if 1 in (halves or (1,)):
+            early_copy(p, 1, f, x_peer).start()
+            early_copy(p, 2, f, y_peer).start()
 
     def act_relay(p):
-        early_copy(p, 0, x_peer, x_peer).wait_recv()
+        early_pair(p, 0).wait_recv()
         early_copy(p, 4, x_peer, y_peer).start()
-        early_copy(p, 3, y_peer, y_peer).wait_recv()
         early_copy(p, 5, y_peer, x_peer).start()
 
     def early_all(k, sem):
@@ -266,10 +273,10 @@
         r = wide[k].at[pl.ds(0, owners)]
         return remote(r, r, early_send.at[k], early_rest.at[k], fs=x_peer)
 
-    def early_pair(p):
+    def early_pair(p, i):
         k, _, size = pairs[p]
         r = wide[k].at[0, pl.ds(0, 2 * size)]
-        return remote(r, r, early_send.at[k], early_recv.at[p, 2], fs=x_peer)
+        return remote(r, r, early_send.at[k], early_recv.at[p, i], fs=x_peer)
 
     def act_open(k):
         loads[1 + k].wait()
@@ -495,7 +502,7 @@
 
     def act_last(p, to):
         for q in range(p, to + 1):
-            early_pair(q).wait_recv()
+            early_pair(q, 1).wait_recv()
         k, at, _ = pairs[p]
         form(k, diag, at, pairs[to][1] + 2 * pairs[to][2] - at)
 
@@ -522,12 +529,12 @@
         top=act_top, code=act_code, open=act_open, join=act_join, relay=act_relay, own=act_own,
         total=act_total, project=act_project, moment=act_moment, spread=act_spread, tally=act_tally,
         direction=act_direction, finish=act_finish, settle=act_settle, send=act_send,
-        form=act_form, last=act_last, arrive=act_arrive, drain=act_drain,
+        form=act_form, share=act_share, last=act_last, arrive=act_arrive, drain=act_drain,
     )
     ramp = SKEW * (zs - 1)
     steps = count + ramp
     todo = [(step, 0, z_step, (step,)) for step in range(steps)]
-    todo += [(at, 1, acts[name], args) for at, name, *args in JOINS if n == 4 or name in ("open", "join")]
+    todo += [(at, 1, acts[name], args) for at, name, *args in JOINS if n == 4 or name in ("share", "open", "join")]
     if n == 4:
         todo += [(ramp + at, 2, acts[name], args) for at, name, *args in TAIL]
     else:
@@ -600,8 +607,10 @@
         + [dma(16), dma(2), dma(2, count), dma(2), dma(6 + SHARES)]
         + [dma(3)] * 3
         + [dma(3, 3)]
-        + [dma(3)] * 5
-        + [dma(3), dma(3), dma(max(len(pairs), 1), 3)] + [dma(3)] * 3
+        + [dma(3)] * 4
+        + [dma(1 if n == 4 else 3)] * 2
+        + [dma(3), dma(max(len(pairs), 1), 2)]
+        + [dma(3)] * 3
     )
     held = pl.pallas_call(
         functools.partial(kernel, n, tp),

time: 58.8 us -> 58.6 us (level)
  no operation moved by 1% of the time
where the time goes in v6:
time: 58.6 us; the launch traced here: 58.5 us
  Pallas kernels  57.8 us (99%)
  between operations  0.66 us (1%)
    pallas_call x1, Pallas kernels, shards(): pl.pallas_call(functools.partial(kernel, n, tp), out_shape=outs, in_specs...  54 us
    pallas_call x1, Pallas kernels, shards(): pl.pallas_call(emit, out_shape=[jax.ShapeDtypeStruct(a.shape, a.dtype) fo...  3.84 us

profile of v6, /device:TPU:0, one launch (start us, length us, event | category | flops | bytes accessed | tf_op | source)
XLA Modules:
  0.0 58.5 jit_solution(13561769997380628943)
XLA Ops:
  0.7 54.0 %shard_map.271 = (f32[512,512]{1,0:T(8,128)S(1)}, f32[512,512]{1,0:T(8,128)S(1)}, f32[32,512]{1,0:T(8,128)S(1)}, f32[32,512]{1,0:T(8,128)S(1)}, bf16[2048,512]{1...) custom-call(bf16[2048,256]{1,0:T(8,128)(2,1)} %refs_0_.1, ...), custom_call_target="tpu_custom_call" | custom-call | tf_op jit(solution)/shard_map/pallas_call | solution.py:615
  54.6 3.8 %shard_map.272 = (f32[512,512]{1,0:T(8,128)}, f32[512,512]{1,0:T(8,128)}, f32[32,512]{1,0:T(8,128)}, f32[32,512]{1,0:T(8,128)}, bf16[2048,512]{1,0:T(8,128)(2,1)...) custom-call(f32[512,512]{1,0:T(8,128)S(1)} %get-tuple-element.30.ref, ...), custom_call_target="tpu_custom_call" | custom-call | tf_op jit(solution)/shard_map/pallas_call | solution.py:625
